TPU v7x, 32 devices: a whole 2x2x4 slice. The times are simulated.
32 devices in a mesh: sp: 8 (over z, y), tp: 4 (over x, core).
Axes of the slice: x: 2, y: 2, z: 4, core: 2. Of those that a mesh axis runs over, the one named last changes fastest.
Arguments:
- out_grad: bfloat16 [1024, 2048], P('sp'), may hold values from -6 to 6
- residual: bfloat16 [1024, 2048], P('sp'), may hold values from -6 to 6
- routes: int32 [1024, 2], P('sp'), may hold values from 0 to 3, all different within a row; in each aligned block of 128 rows (0 to 127, 128 to 255, ...) at most 80 rows name the same one
- route_weights: float32 [1024, 2], P('sp'), may hold values from 0.15 to 0.85, as said below
- w_gate: bfloat16 [8, 2048, 2048], P('sp', None, 'tp'), may hold values from -0.125 to 0.125
- w_up: bfloat16 [8, 2048, 2048], P('sp', None, 'tp'), may hold values from -0.125 to 0.125
- w_down: bfloat16 [8, 2048, 2048], P('sp', 'tp'), may hold values from -0.09375 to 0.09375
- out_gate: bfloat16 [1024, 1024], P('sp', 'tp'), may hold values from -6 to 6
- in_gate: bfloat16 [1024, 1024], P('sp', 'tp'), may hold values from -6 to 6
- conv_input: bfloat16 [1024, 1024], P('sp', 'tp'), may hold values from -6 to 6
- conv_out: bfloat16 [1024, 1024], P('sp', 'tp'), may hold values from -6 to 6
- conv_taps: float32 [3, 1024], P(None, 'tp'), may hold values from -3.5 to 3.5
- w_out: bfloat16 [1024, 2048], P('tp'), may hold values from -0.1875 to 0.1875
Outputs:
- grad_resid: bfloat16 [1024, 2048], P('sp')
- grad_up: bfloat16 [8, 2048, 2048], P('sp', None, 'tp')
- grad_down: bfloat16 [8, 2048, 2048], P('sp', 'tp')
- grad_out_gate: bfloat16 [1024, 1024], P('sp', 'tp')
- grad_in_gate: bfloat16 [1024, 1024], P('sp', 'tp')
- grad_conv_input: bfloat16 [1024, 1024], P('sp', 'tp')
- grad_w_out: float32 [2048, 1024], P('sp', 'tp')
Inputs may be any that keep to these rules, and one draw needn't show every extreme that they name: `routes`: each row names 2 different experts. In the rows of one index of sp no expert is named more than 80 times, a bound that some block reaches. `route_weights`: the two weights of a row sum to one.
All inputs are finite; a program needn't handle non-finite values.
Results may differ from a plain program's by a relative error of at most 0.013.
Values may be sent and summed in bfloat16 or wider, within the bound.
A program may use at most 128 MiB of HBM per device.

v0:
```python
import functools

import jax
import jax.numpy as jnp
from jax import lax
from jax.experimental import pallas as pl
from jax.experimental.pallas import tpu as pltpu
from jax.sharding import PartitionSpec as P

epsilon = 1e-06


def with_halo(cells, sides, width):
    for axis, dim in sides:
        count = lax.axis_size(axis)
        ends = count - 1
        head = lax.slice_in_dim(cells, 0, width, axis=dim)
        tail = lax.slice_in_dim(cells, cells.shape[dim] - width, cells.shape[dim], axis=dim)
        cells = jnp.concatenate(
            [
                lax.ppermute(tail, axis, [(i, (i + 1) % count) for i in range(ends)]),
                cells,
                lax.ppermute(head, axis, [((i + 1) % count, i) for i in range(ends)]),
            ],
            axis=dim,
        )
    return cells


def per_device_general(
    out_grad,
    residual,
    routes,
    route_weights,
    w_gate,
    w_up,
    w_down,
    out_gate,
    in_gate,
    conv_input,
    conv_out,
    conv_taps,
    w_out,
):
    tok_rows = out_grad.shape[0]
    features = out_grad.shape[1]
    top_count = routes.shape[1]
    slices = lax.axis_size("sp")
    experts = slices // 2
    capacity = 5 * tok_rows // slices
    n_assign = tok_rows * top_count
    resid_f32 = residual.astype(jnp.float32)
    inv_rms = lax.rsqrt(jnp.mean(resid_f32 * resid_f32, axis=-1, keepdims=True) + epsilon)
    unit_rows = resid_f32 * inv_rms
    normed = unit_rows.astype(jnp.bfloat16)
    weighted = (
        (route_weights[:, :, None] * out_grad.astype(jnp.float32)[:, None, :])
        .astype(jnp.bfloat16)
        .reshape(n_assign, features)
    )
    flat_routes = routes.reshape(-1)
    onehot = (flat_routes[:, None] == jnp.arange(experts, dtype=jnp.int32)[None, :]).astype(
        jnp.int32
    )
    slot_rank = jnp.sum((jnp.cumsum(onehot, axis=0) - onehot) * onehot, axis=1)
    slot_index = flat_routes * capacity + slot_rank
    slot_table = (
        jnp.full((experts * capacity,), n_assign, jnp.int32)
        .at[slot_index]
        .set(jnp.arange(n_assign, dtype=jnp.int32))
    )
    filled = slot_table < n_assign
    safe_index = jnp.where(filled, slot_table, 0)
    send_rows = jnp.where(
        filled[:, None], normed[safe_index // top_count], jnp.zeros((), jnp.bfloat16)
    )
    send_grads = jnp.where(filled[:, None], weighted[safe_index], jnp.zeros((), jnp.bfloat16))
    outgoing = jnp.stack([send_rows, send_grads])
    doubled = jnp.repeat(outgoing.reshape(2, experts, capacity, features), 2, axis=1)
    arrived = lax.all_to_all(doubled, "sp", split_axis=1, concat_axis=1, tiled=True)
    expert_rows = arrived[0].reshape(slices * capacity, features)
    expert_grads = arrived[1].reshape(slices * capacity, features)
    gate_local = w_gate[0]
    up_local = w_up[0]
    down_local = w_down[0]
    pre_gate = jnp.dot(expert_rows, gate_local, preferred_element_type=jnp.float32)
    pre_up = jnp.dot(expert_rows, up_local, preferred_element_type=jnp.float32)
    sigmoid_gate = jax.nn.sigmoid(pre_gate)
    activated = pre_gate * sigmoid_gate
    hidden = (activated * pre_up).astype(jnp.bfloat16)
    d_hidden = lax.dot_general(
        expert_grads, down_local, (((1,), (1,)), ((), ())), preferred_element_type=jnp.float32
    )
    grad_down = lax.dot_general(
        hidden, expert_grads, (((0,), (0,)), ((), ())), preferred_element_type=jnp.float32
    ).astype(jnp.bfloat16)
    d_gate = (d_hidden * pre_up * sigmoid_gate * (1.0 + pre_gate * (1.0 - sigmoid_gate))).astype(
        jnp.bfloat16
    )
    d_up = (d_hidden * activated).astype(jnp.bfloat16)
    grad_up = lax.dot_general(
        expert_rows, d_up, (((0,), (0,)), ((), ())), preferred_element_type=jnp.float32
    ).astype(jnp.bfloat16)
    partial_value = lax.dot_general(
        d_gate, gate_local, (((1,), (1,)), ((), ())), preferred_element_type=jnp.float32
    )
    partial_value = partial_value + lax.dot_general(
        d_up, up_local, (((1,), (1,)), ((), ())), preferred_element_type=jnp.float32
    )
    partial_value = partial_value.astype(jnp.bfloat16).reshape(slices, capacity, features)
    summed = lax.psum_scatter(partial_value, "tp", scatter_dimension=2, tiled=True).astype(
        jnp.float32
    )
    returned = lax.all_to_all(
        summed.astype(jnp.bfloat16), "sp", split_axis=0, concat_axis=0, tiled=True
    )
    columns = returned.shape[2]
    flat_back = returned.reshape(slices * capacity, columns)
    first_index = 2 * flat_routes * capacity + slot_rank
    contrib = flat_back[first_index].astype(jnp.float32) + flat_back[first_index + capacity].astype(
        jnp.float32
    )
    d_normed = jnp.sum(contrib.reshape(tok_rows, top_count, columns), axis=1)
    col_start = lax.axis_index("tp") * columns
    unit_part = lax.dynamic_slice_in_dim(unit_rows, col_start, columns, 1)
    grad_part = lax.dynamic_slice_in_dim(out_grad, col_start, columns, 1).astype(jnp.float32)
    row_dots = lax.psum(jnp.sum(unit_part * d_normed, axis=-1), "tp")
    row_mean = row_dots[:, None] / features
    resid_part = (grad_part + inv_rms * (d_normed - unit_part * row_mean)).astype(jnp.bfloat16)
    grad_resid = lax.all_gather(resid_part, "tp", axis=1, tiled=True)
    d_mix = lax.dot_general(
        grad_resid, w_out, (((1,), (1,)), ((), ())), preferred_element_type=jnp.float32
    )
    conv_f32 = conv_out.astype(jnp.float32)
    gate_f32 = out_gate.astype(jnp.float32)
    grad_out_gate = (d_mix * conv_f32).astype(jnp.bfloat16)
    d_conv = d_mix * gate_f32
    padded = with_halo(d_conv.astype(jnp.bfloat16), (("sp", 0),), 1).astype(d_conv.dtype)
    d_inner = conv_taps[0] * padded[2:] + conv_taps[1] * padded[1:-1] + conv_taps[2] * padded[:-2]
    grad_in_gate = (d_inner * conv_input.astype(jnp.float32)).astype(jnp.bfloat16)
    grad_conv_input = (d_inner * in_gate.astype(jnp.float32)).astype(jnp.bfloat16)
    mixed = (gate_f32 * conv_f32).astype(jnp.bfloat16)
    grad_w_out = lax.psum_scatter(
        lax.dot_general(
            grad_resid, mixed, (((0,), (0,)), ((), ())), preferred_element_type=jnp.float32
        ),
        "sp",
        scatter_dimension=0,
        tiled=True,
    )
    return (
        grad_resid,
        grad_up[None],
        grad_down[None],
        grad_out_gate,
        grad_in_gate,
        grad_conv_input,
        grad_w_out,
    )


MESH = pl.DeviceIdType.MESH
BF16 = jnp.bfloat16
F32 = jnp.float32
VMEM_LIMIT = 60 * 1024 * 1024


def place():
    sp, tp = lax.axis_index("sp"), lax.axis_index("tp")
    return sp, tp, lax.div(sp, 2), lax.rem(sp, 2), lax.div(tp, 2), lax.rem(tp, 2)


def greet(peers):
    barrier = pltpu.get_barrier_semaphore()
    for peer in peers:
        pl.semaphore_signal(barrier, inc=1, device_id=peer, device_id_type=MESH)
    return lambda: pl.semaphore_wait(barrier, len(peers))


def columns_of(index, width):
    return pl.ds(pl.multiple_of(index * width, width), width)


def rows_of(index, height):
    return pl.ds(pl.multiple_of(index * height, height), height)


def dispatch_kernel(
    slices, cap, rt, rw, resid, og, gate_hbm, up_hbm, down_hbm,
    rows, grads, hidden, d_gate, d_up, sel,
    send_rows, send_grads, gate, up, down, send_sem, recv_sem, local_sem,
):
    sp, tp, z, y, x, c = place()
    pairs = slices // 2
    tok, features = resid.shape
    width = features // 4
    sibling = (sp, 2 * x + 1 - c)
    x_peer = (sp, 2 * (1 - x) + c)
    y_peer = (2 * z + 1 - y, tp)
    z_peers = [(2 * lax.rem(z + k, pairs) + y, tp) for k in range(1, pairs)]
    ready = greet(z_peers + [sibling, x_peer, y_peer])
    weights = [
        pltpu.make_async_copy(src, dst, local_sem.at[2 + n])
        for n, (src, dst) in enumerate(((gate_hbm, gate), (up_hbm, up), (down_hbm, down)))
    ]
    for copy in weights:
        copy.start()

    grid_r = lax.broadcasted_iota(jnp.int32, (tok, tok), 0)
    grid_c = lax.broadcasted_iota(jnp.int32, (tok, tok), 1)
    earlier = (grid_r < grid_c).astype(F32).astype(BF16)
    slot = lax.broadcasted_iota(jnp.int32, (cap, tok), 0).astype(F32)
    r32 = resid[...].astype(F32)
    inv_rms = lax.rsqrt(jnp.mean(r32 * r32, axis=-1, keepdims=True) + epsilon)
    mine = columns_of(tp, width)
    normed = (resid[:, mine].astype(F32) * inv_rms).astype(BF16)
    cot = og[:, mine]
    for e in range(pairs):
        named = (rt[...] == e).astype(F32)
        mask = jnp.sum(named, axis=0, keepdims=True)
        weight = jnp.sum(named * rw[...], axis=0, keepdims=True)
        rank = jnp.dot(
            jnp.broadcast_to(mask, (8, tok)).astype(BF16), earlier, preferred_element_type=F32
        )[0:1]
        pick = jnp.where((rank == slot) & (mask > 0.5), 1.0, 0.0)
        slot_weight = jnp.sum(pick * weight, axis=1, keepdims=True)
        pick = pick.astype(BF16)
        here = slice(e * cap, (e + 1) * cap)
        sel[here, :] = pick
        send_rows[here, :] = jnp.dot(pick, normed, preferred_element_type=F32).astype(BF16)
        send_grads[here, :] = (
            slot_weight * jnp.dot(pick, cot, preferred_element_type=F32)
        ).astype(BF16)
    ready()

    started = []

    def send(n, src, dst, peer):
        copy = pltpu.make_async_remote_copy(
            src_ref=src, dst_ref=dst, send_sem=send_sem.at[n], recv_sem=recv_sem.at[n],
            device_id=peer, device_id_type=MESH,
        )
        copy.start()
        started.append(copy)
        return copy

    ours = ((send_rows, rows), (send_grads, grads))

    def block(pair, yy, xx, cc):
        return (rows_of(2 * pair + yy, cap), columns_of(2 * xx + cc, width))

    arriving = {}
    home = block(z, y, x, c)
    for k in range(1, pairs):
        far = lax.rem(z - k + pairs, pairs)
        for a, (src, dst) in enumerate(ours):
            arriving[k, a] = send(
                16 * pairs + 2 * k + a, src.at[rows_of(far, cap), :], dst.at[home],
                (2 * far + y, tp),
            )
    locals_ = []
    for a, (src, dst) in enumerate(ours):
        copy = pltpu.make_async_copy(src.at[rows_of(z, cap), :], dst.at[home], local_sem.at[a])
        copy.start()
        locals_.append(copy)
    for copy in locals_:
        copy.wait()

    def spread(k):
        pair = lax.rem(z + k, pairs)
        at = block(pair, y, x, c)
        out = {}
        for a, (_, dst) in enumerate(ours):
            out["x", a] = send(16 * k + a, dst.at[at], dst.at[at], x_peer)
            out["y", a] = send(16 * k + 2 + a, dst.at[at], dst.at[at], y_peer)
        for a, (_, dst) in enumerate(ours):
            out["s", a] = send(16 * k + 4 + a, dst.at[at], dst.at[at], sibling)
        return out

    def forward(k, out):
        pair = lax.rem(z + k, pairs)
        got_x = block(pair, y, 1 - x, c)
        got_y = block(pair, 1 - y, x, c)
        out["x", 0].wait_recv()
        out["dy"] = send(16 * k + 6, rows.at[got_x], rows.at[got_x], y_peer)
        out["y", 1].wait_recv()
        out["dx"] = send(16 * k + 7, grads.at[got_y], grads.at[got_y], x_peer)
        out["x", 1].wait_recv()
        out["y", 0].wait_recv()
        for a, (_, dst) in enumerate(ours):
            out["sx", a] = send(16 * k + 8 + a, dst.at[got_x], dst.at[got_x], sibling)
            out["sy", a] = send(16 * k + 10 + a, dst.at[got_y], dst.at[got_y], sibling)

    def finish(k, out):
        pair = lax.rem(z + k, pairs)
        got = block(pair, 1 - y, 1 - x, c)
        out["dy"].wait_recv()
        out["sd", 0] = send(16 * k + 12, rows.at[got], rows.at[got], sibling)
        out["dx"].wait_recv()
        out["sd", 1] = send(16 * k + 13, grads.at[got], grads.at[got], sibling)

    def experts(k, out):
        for kind in ("s", "sx", "sy", "sd"):
            for a in range(2):
                out[kind, a].wait_recv()
        at = rows_of(lax.rem(z + k, pairs), 2 * cap)
        pre_gate = jnp.dot(rows[at, :], gate[...], preferred_element_type=F32)
        pre_up = jnp.dot(rows[at, :], up[...], preferred_element_type=F32)
        d_hidden = lax.dot_general(
            grads[at, :], down[...], (((1,), (1,)), ((), ())), preferred_element_type=F32
        )
        sigmoid_gate = jax.nn.sigmoid(pre_gate)
        activated = pre_gate * sigmoid_gate
        hidden[at, :] = (activated * pre_up).astype(BF16)
        d_gate[at, :] = (
            d_hidden * pre_up * sigmoid_gate * (1.0 + pre_gate * (1.0 - sigmoid_gate))
        ).astype(BF16)
        d_up[at, :] = (d_hidden * activated).astype(BF16)

    outs = []
    for k in range(pairs):
        if k:
            for a in range(2):
                arriving[k, a].wait_recv()
        outs.append(spread(k))
        if k:
            forward(k - 1, outs[k - 1])
        if k > 1:
            finish(k - 2, outs[k - 2])
    for copy in weights:
        copy.wait()
    for k in range(pairs - 2):
        experts(k, outs[k])
        if k == 0:
            forward(pairs - 1, outs[-1])
            finish(pairs - 2, outs[-2])
    finish(pairs - 1, outs[-1])
    experts(pairs - 2, outs[-2])
    experts(pairs - 1, outs[-1])
    for copy in started:
        copy.wait_send()


def dispatch(slices, cap, rt, rw, resid, og, gate, up, down):
    features, tok = resid.shape[1], resid.shape[0]
    pairs = slices // 2
    vmem = pl.BlockSpec(memory_space=pltpu.VMEM)
    sems = 18 * pairs
    wide = jax.ShapeDtypeStruct((slices * cap, features), BF16)
    narrow = jax.ShapeDtypeStruct((slices * cap, gate.shape[1]), BF16)
    return pl.pallas_call(
        functools.partial(dispatch_kernel, slices, cap),
        out_shape=(
            wide, wide, narrow, narrow, narrow, jax.ShapeDtypeStruct((pairs * cap, tok), BF16),
        ),
        in_specs=[vmem] * 4 + [pl.BlockSpec(memory_space=pl.ANY)] * 3,
        out_specs=[vmem] * 6,
        scratch_shapes=[
            pltpu.VMEM((pairs * cap, features // 4), BF16),
            pltpu.VMEM((pairs * cap, features // 4), BF16),
            pltpu.VMEM(gate.shape, BF16),
            pltpu.VMEM(up.shape, BF16),
            pltpu.VMEM(down.shape, BF16),
            pltpu.SemaphoreType.DMA((sems,)),
            pltpu.SemaphoreType.DMA((sems,)),
            pltpu.SemaphoreType.DMA((5,)),
        ],
        compiler_params=pltpu.CompilerParams(
            collective_id=0, has_side_effects=True, vmem_limit_bytes=VMEM_LIMIT
        ),
        name="dispatch",
    )(rt, rw, resid, og, gate, up, down)


def tail_kernel(
    slices, cap, d_gate, d_up, sel, resid, og, ogate, cout, wout, gate_hbm, up_hbm,
    gresid, d_mix_out, edge_in, grx, mixed,
    part, gate, up, sib, pairsum, plane, zsend, ret, dnq, dn, edge_out,
    send_sem, recv_sem, local_sem,
):
    sp, tp, z, y, x, c = place()
    pairs = slices // 2
    tok, features = resid.shape
    width = features // 4
    sibling = (sp, 2 * x + 1 - c)
    x_peer = (sp, 2 * (1 - x) + c)
    x_other = (sp, 2 * (1 - x) + 1 - c)
    y_peer = (2 * z + 1 - y, tp)
    diagonal = (2 * z + 1 - y, 2 * (1 - x) + c)
    sp_peers = [(lax.rem(sp + k, slices), tp) for k in range(1, slices)]
    ready = greet(sp_peers + [sibling, x_peer, x_other, diagonal])
    weights = [
        pltpu.make_async_copy(src, dst, local_sem.at[n])
        for n, (src, dst) in enumerate(((gate_hbm, gate), (up_hbm, up)))
    ]
    for copy in weights:
        copy.start()
    own = rows_of(sp, tok)
    mixed[own, :] = (ogate[...].astype(F32) * cout[...].astype(F32)).astype(BF16)
    ready()
    started = []

    def send(n, src, dst, peer):
        copy = pltpu.make_async_remote_copy(
            src_ref=src, dst_ref=dst, send_sem=send_sem.at[n], recv_sem=recv_sem.at[n],
            device_id=peer, device_id_type=MESH,
        )
        copy.start()
        started.append(copy)
        return copy

    first = 8 * pairs + 3 + 2 * slices + 2
    mixed_copies = [
        send(first + n, mixed.at[own, :], mixed.at[own, :], peer)
        for n, peer in enumerate(sp_peers)
    ]
    for copy in weights:
        copy.wait()
    order = list(range(1, pairs)) + [0]
    halves = {}
    across_units = (((1,), (1,)), ((), ()))
    for k in order:
        at = rows_of(lax.rem(z + k, pairs), 2 * cap)
        part[at, :] = (
            lax.dot_general(d_gate[at, :], gate[...], across_units, preferred_element_type=F32)
            + lax.dot_general(d_up[at, :], up[...], across_units, preferred_element_type=F32)
        ).astype(BF16)
        for h in range(2):
            halves[k, h] = send(
                8 * k + h, part.at[at, columns_of(2 * h + 1 - c, width)], sib.at[h, at, :], sibling
            )
    moved = {}
    for k in order:
        pair = lax.rem(z + k, pairs)
        at = rows_of(pair, 2 * cap)
        for h in range(2):
            halves[k, h].wait_recv()
            pairsum[h, at, :] = (
                part[at, columns_of(2 * h + c, width)].astype(F32) + sib[h, at, :].astype(F32)
            ).astype(BF16)
        same, other = rows_of(2 * pair + y, cap), rows_of(2 * pair + 1 - y, cap)
        slots = rows_of(pair, cap)
        moved[k] = [
            send(8 * k + 2, pairsum.at[1 - x, same, :], plane.at[0, slots, :], x_peer),
            send(8 * k + 3, pairsum.at[x, other, :], plane.at[1, slots, :], y_peer),
            send(8 * k + 4, pairsum.at[1 - x, other, :], plane.at[2, slots, :], diagonal),
        ]
    back = []
    for k in order:
        pair = lax.rem(z + k, pairs)
        slots = rows_of(pair, cap)
        for copy in moved[k]:
            copy.wait_recv()
        total = (
            pairsum[x, rows_of(2 * pair + y, cap), :].astype(F32)
            + plane[0, slots, :].astype(F32)
            + plane[1, slots, :].astype(F32)
            + plane[2, slots, :].astype(F32)
        ).astype(BF16)
        if k:
            zsend[slots, :] = total
            back.append(
                send(8 * k + 5, zsend.at[slots, :], ret.at[rows_of(z, cap), :], (2 * pair + y, tp))
            )
        else:
            ret[slots, :] = total
    r32 = resid[...].astype(F32)
    inv_rms = lax.rsqrt(jnp.mean(r32 * r32, axis=-1, keepdims=True) + epsilon)
    for copy in back:
        copy.wait_recv()
    first = 8 * pairs
    quarter = lax.dot_general(
        sel[...], ret[...], (((0,), (0,)), ((), ())), preferred_element_type=F32
    ).astype(BF16)
    dnq[...] = quarter
    mine = columns_of(tp, width)
    dn[:, mine] = quarter
    shares = [
        send(first + n, dnq, dn.at[:, mine], peer)
        for n, peer in enumerate((x_other, x_peer, sibling))
    ]
    for copy in shares:
        copy.wait_recv()
    unit = r32 * inv_rms
    d_normed = dn[...].astype(F32)
    row_mean = jnp.mean(unit * d_normed, axis=-1, keepdims=True)
    gresid[...] = (og[...].astype(F32) + inv_rms * (d_normed - unit * row_mean)).astype(BF16)
    share = features // slices
    half = tok // 2
    first += 3
    across = [
        send(
            first + n, gresid.at[rows_of(c, half), columns_of(peer[0], share)],
            grx.at[rows_of(2 * sp + c, half), :], peer,
        )
        for n, peer in enumerate(sp_peers)
    ]
    d_mix = lax.dot_general(
        gresid[...], wout[...], (((1,), (1,)), ((), ())), preferred_element_type=F32
    )
    d_conv = d_mix * ogate[...].astype(F32)
    edge_out[0] = d_conv[tok - 8 :]
    edge_out[1] = d_conv[:8]
    first += 2 * slices
    edges = [
        send(first, edge_out.at[0], edge_in.at[0], sp_peers[0]),
        send(first + 1, edge_out.at[1], edge_in.at[1], sp_peers[-1]),
    ]
    d_mix_out[...] = d_mix
    grx[own, :] = gresid[:, columns_of(sp, share)]
    first -= slices
    passed = []
    for n in range(slices - 1):
        across[n].wait_recv()
        got = grx.at[rows_of(2 * lax.rem(sp + slices - 1 - n, slices) + c, half), :]
        passed.append(send(first + n, got, got, sibling))
    for copy in edges + passed + mixed_copies:
        copy.wait_recv()
    for copy in started:
        copy.wait_send()


def finish_kernel(
    gresid_in, d_mix, edges, grx, mixed, ogate, igate, cin, cout, taps,
    gresid, gogate, gigate, gcin, gwout,
):
    sp, slices = lax.axis_index("sp"), lax.axis_size("sp")
    tok = gresid.shape[0]
    gresid[...] = gresid_in[...]
    gogate[...] = (d_mix[...] * cout[...].astype(F32)).astype(BF16)
    d_conv = d_mix[...] * ogate[...].astype(F32)
    before = jnp.where(sp > 0, edges[0, 7:8, :], 0.0)
    after = jnp.where(sp < slices - 1, edges[1, 0:1, :], 0.0)
    at = lax.broadcasted_iota(jnp.int32, d_conv.shape, 0)
    later = jnp.where(at == tok - 1, after, pltpu.roll(d_conv, tok - 1, 0))
    former = jnp.where(at == 0, before, pltpu.roll(d_conv, 1, 0))
    d_inner = taps[0:1, :] * later + taps[1:2, :] * d_conv + taps[2:3, :] * former
    gigate[...] = (d_inner * cin[...].astype(F32)).astype(BF16)
    gcin[...] = (d_inner * igate[...].astype(F32)).astype(BF16)
    gwout[...] = lax.dot_general(
        grx[...], mixed[...], (((0,), (0,)), ((), ())), preferred_element_type=F32
    )


def tail(slices, cap, d_gate, d_up, sel, resid, og, ogate, cout, wout, gate, up):
    tok, features = resid.shape
    channels = ogate.shape[1]
    pairs = slices // 2
    width = features // 4
    vmem = pl.BlockSpec(memory_space=pltpu.VMEM)
    sems = 8 * pairs + 3 + 3 * slices + 2
    return pl.pallas_call(
        functools.partial(tail_kernel, slices, cap),
        out_shape=(
            jax.ShapeDtypeStruct((tok, features), BF16),
            jax.ShapeDtypeStruct((tok, channels), F32),
            jax.ShapeDtypeStruct((2, 8, channels), F32),
            jax.ShapeDtypeStruct((slices * tok, features // slices), BF16),
            jax.ShapeDtypeStruct((slices * tok, channels), BF16),
        ),
        in_specs=[vmem] * 8 + [pl.BlockSpec(memory_space=pl.ANY)] * 2,
        out_specs=[vmem] * 5,
        scratch_shapes=[
            pltpu.VMEM((slices * cap, features), BF16),
            pltpu.VMEM(gate.shape, BF16),
            pltpu.VMEM(up.shape, BF16),
            pltpu.VMEM((2, slices * cap, width), BF16),
            pltpu.VMEM((2, slices * cap, width), BF16),
            pltpu.VMEM((3, pairs * cap, width), BF16),
            pltpu.VMEM((pairs * cap, width), BF16),
            pltpu.VMEM((pairs * cap, width), BF16),
            pltpu.VMEM((tok, width), BF16),
            pltpu.VMEM((tok, features), BF16),
            pltpu.VMEM((2, 8, channels), F32),
            pltpu.SemaphoreType.DMA((sems,)),
            pltpu.SemaphoreType.DMA((sems,)),
            pltpu.SemaphoreType.DMA((2,)),
        ],
        compiler_params=pltpu.CompilerParams(
            collective_id=1, has_side_effects=True, vmem_limit_bytes=VMEM_LIMIT
        ),
        name="tail",
    )(d_gate, d_up, sel, resid, og, ogate, cout, wout, gate, up)


def finish(tail_out, ogate, igate, cin, cout, taps):
    gresid, _, _, grx, _ = tail_out
    vmem = pl.BlockSpec(memory_space=pltpu.VMEM)
    small = jax.ShapeDtypeStruct(ogate.shape, BF16)
    return pl.pallas_call(
        finish_kernel,
        out_shape=(
            jax.ShapeDtypeStruct(gresid.shape, BF16), small, small, small,
            jax.ShapeDtypeStruct((grx.shape[1], ogate.shape[1]), F32),
        ),
        in_specs=[vmem] * 10,
        out_specs=[vmem] * 5,
        name="finish",
    )(*tail_out, ogate, igate, cin, cout, taps)


def per_device(
    out_grad, residual, routes, route_weights, w_gate, w_up, w_down,
    out_gate, in_gate, conv_input, conv_out, conv_taps, w_out,
):
    slices = lax.axis_size("sp")
    cap = 5 * out_grad.shape[0] // slices
    gate_local, up_local, down_local = w_gate[0], w_up[0], w_down[0]
    expert_rows, expert_grads, hidden, d_gate, d_up, sel = dispatch(
        slices, cap, routes.T, route_weights.T, residual, out_grad,
        gate_local, up_local, down_local,
    )
    grad_down = lax.dot_general(
        hidden, expert_grads, (((0,), (0,)), ((), ())), preferred_element_type=F32
    ).astype(BF16)
    grad_up = lax.dot_general(
        expert_rows, d_up, (((0,), (0,)), ((), ())), preferred_element_type=F32
    ).astype(BF16)
    tail_out = tail(
        slices, cap, d_gate, d_up, sel, residual, out_grad, out_gate, conv_out, w_out,
        gate_local, up_local,
    )
    grad_resid, grad_out_gate, grad_in_gate, grad_conv_input, grad_w_out = finish(
        tail_out, out_gate, in_gate, conv_input, conv_out, conv_taps
    )
    return (
        grad_resid, grad_up[None], grad_down[None], grad_out_gate, grad_in_gate,
        grad_conv_input, grad_w_out,
    )


def fits_kernels(mesh, tokens):
    slices = mesh.shape["sp"]
    rows = tokens // slices
    return mesh.shape["tp"] == 4 and slices >= 4 and (5 * rows // slices) % 16 == 0


def on_device(mesh, out_grad, *rest):
    tokens = out_grad.shape[0] * mesh.shape["sp"]
    body = per_device if fits_kernels(mesh, tokens) else per_device_general
    return body(out_grad, *rest)


def solution(mesh):
    in_specs = (
        P("sp", None),
        P("sp", None),
        P("sp", None),
        P("sp", None),
        P("sp", None, "tp"),
        P("sp", None, "tp"),
        P("sp", "tp", None),
        P("sp", "tp"),
        P("sp", "tp"),
        P("sp", "tp"),
        P("sp", "tp"),
        P(None, "tp"),
        P("tp", None),
    )
    out_specs = (
        P("sp", None),
        P("sp", None, "tp"),
        P("sp", "tp", None),
        P("sp", "tp"),
        P("sp", "tp"),
        P("sp", "tp"),
        P("sp", "tp"),
    )
    return jax.shard_map(
        functools.partial(on_device, mesh), mesh=mesh, in_specs=in_specs, out_specs=out_specs, check_vma=False
    )
```

profile of v0, /device:TPU:0, one launch (start us, length us, event | category | flops | bytes accessed | tf_op | source)
XLA Modules:
  0.0 98.5 jit_solution(7953111886948021738)
XLA Ops:
  0.6 44.6 %dispatch.1 = (bf16[640,2048]{1,0:T(8,128)(2,1)}, bf16[640,2048]{1,0:T(8,128)(2,1)}, bf16[640,512]{1,0:T(8,128)(2,1)}, bf16[640,512]{1,0:T(8,128)(2,1)}, bf16[64...) custom-call(s32[2,128]{1,0:T(2,128)} %bitcast.18, f32[2,128]{1,0:T(2,128)} %bitcast.19, bf16[128,2048]{1,0:T(8,128)(2,1)} %resid.3, ...), custom_call_target="tpu_custom_call" | custom-call | tf_op jit(solution)/shard_map/dispatch/pallas_call | solution.py:351
  45.3 0.0 copy-start.2
  45.3 0.0 copy-start.3
  45.3 44.0 %tail.1 = (bf16[128,2048]{1,0:T(8,128)(2,1)}, f32[128,256]{1,0:T(8,128)}, f32[2,8,256]{2,1,0:T(8,128)}, bf16[1024,256]{1,0:T(8,128)(2,1)}, bf16[1024,256]{1,0:T(8,128)(2,1)}) custom-call(bf16[640,512]{1,0:T(8,128)(2,1)} %get-tuple-element.23.d_gate, bf16[640,512]{1,0:T(8,128)(2,1)} %get-tuple-element.24.d_up, bf16[320,128]{1,0:T(8,128)(2,1)} %get-tuple-element.25.sel, ...), custom_call_target="tpu_custom_call" | custom-call | tf_op jit(solution)/shard_map/tail/pallas_call | solution.py:552
  89.3 2.8 %finish.1 = (bf16[128,2048]{1,0:T(8,128)(2,1)}, bf16[128,256]{1,0:T(8,128)(2,1)}, bf16[128,256]{1,0:T(8,128)(2,1)}, bf16[128,256]{1,0:T(8,128)(2,1)}, f32[256,256]{1,0:T(8,128)}) custom-call(bf16[128,2048]{1,0:T(8,128)(2,1)} %get-tuple-element.26.gresid_in, f32[128,256]{1,0:T(8,128)} %get-tuple-element.27.d_mix, f32[2,8,256]{2,1,0:T(8,128)} %get-tuple-element.28.edges, ...), custom_call_target="tpu_custom_call" | custom-call | tf_op jit(solution)/shard_map/finish/pallas_call | solution.py:590
  92.1 0.0 copy-done.2
  92.1 0.0 copy-done.3
  92.1 0.0 copy-start
  92.1 0.0 copy-start.1
  92.1 3.2 %fusion = bf16[1,2048,512]{2,1,0:T(8,128)(2,1)} fusion(bf16[640,2048]{1,0:T(8,128)(2,1)S(1)} %copy-done.3, bf16[640,512]{1,0:T(8,128)(2,1)S(1)} %copy-done.2), kind=kOutput, calls=%fused_computation.2 | convolution fusion | flops 1343225856 | bytes 5373952 | tf_op jit(solution)/shard_map/dot_general | solution.py:616
  95.3 0.0 copy-done
  95.3 0.0 copy-done.1
  95.3 3.2 %fusion.1 = bf16[1,512,2048]{2,1,0:T(8,128)(2,1)} fusion(bf16[640,512]{1,0:T(8,128)(2,1)S(1)} %copy-done.1, bf16[640,2048]{1,0:T(8,128)(2,1)S(1)} %copy-done), kind=kOutput, calls=%fused_computation.3 | convolution fusion | flops 1343225856 | bytes 5373952 | tf_op jit(solution)/shard_map/dot_general | solution.py:613
Async XLA Ops:
  45.3 46.8 %copy-start.2 = (bf16[640,512]{1,0:T(8,128)(2,1)S(1)}, bf16[640,512]{1,0:T(8,128)(2,1)}, u32[]{:S(2)}) copy-start(bf16[640,512]{1,0:T(8,128)(2,1)} %get-tuple-element.24.d_up) | copy-start | bytes 1966084
  45.3 46.8 %copy-start.3 = (bf16[640,2048]{1,0:T(8,128)(2,1)S(1)}, bf16[640,2048]{1,0:T(8,128)(2,1)}, u32[]{:S(2)}) copy-start(bf16[640,2048]{1,0:T(8,128)(2,1)} %get-tuple-element.32) | copy-start | bytes 7864324
  92.1 3.2 %copy-start = (bf16[640,2048]{1,0:T(8,128)(2,1)S(1)}, bf16[640,2048]{1,0:T(8,128)(2,1)}, u32[]{:S(2)}) copy-start(bf16[640,2048]{1,0:T(8,128)(2,1)} %get-tuple-element.34) | copy-start | bytes 7864324
  92.1 3.2 %copy-start.1 = (bf16[640,512]{1,0:T(8,128)(2,1)S(1)}, bf16[640,512]{1,0:T(8,128)(2,1)}, u32[]{:S(2)}) copy-start(bf16[640,512]{1,0:T(8,128)(2,1)} %get-tuple-element.33) | copy-start | bytes 1966084
where the time goes:
time: 98.6 us; the launch traced here: 98.5 us
  Pallas kernels  91.4 us (93%)
  matrix products  6.32 us (6%)
    pallas_call x1, Pallas kernels, dispatch(): pl.pallas_call(functools.partial(dispatch_kernel, slices, cap), out_shape...  44.6 us
    pallas_call x1, Pallas kernels, tail(): pl.pallas_call(functools.partial(tail_kernel, slices, cap), out_shape=(ja...  44 us
    dot_general x1, matrix products, per_device(): lax.dot_general(hidden, expert_grads, (((0,), (0,)), ((), ())), preferred...  3.17 us
    dot_general x1, matrix products, per_device(): lax.dot_general(expert_rows, d_up, (((0,), (0,)), ((), ())), preferred_el...  3.15 us
    pallas_call x1, Pallas kernels, finish(): pl.pallas_call(finish_kernel, out_shape=(jax.ShapeDtypeStruct(gresid.shap...  2.77 us

commit v1 on v0

v1 whole, which is shorter than its diff:
```python
import functools

import jax
import jax.numpy as jnp
from jax import lax
from jax.experimental import pallas as pl
from jax.experimental.pallas import tpu as pltpu
from jax.sharding import PartitionSpec as P

epsilon = 1e-06


def with_halo(cells, sides, width):
    for axis, dim in sides:
        count = lax.axis_size(axis)
        ends = count - 1
        head = lax.slice_in_dim(cells, 0, width, axis=dim)
        tail = lax.slice_in_dim(cells, cells.shape[dim] - width, cells.shape[dim], axis=dim)
        cells = jnp.concatenate(
            [
                lax.ppermute(tail, axis, [(i, (i + 1) % count) for i in range(ends)]),
                cells,
                lax.ppermute(head, axis, [((i + 1) % count, i) for i in range(ends)]),
            ],
            axis=dim,
        )
    return cells


def per_device_general(
    out_grad,
    residual,
    routes,
    route_weights,
    w_gate,
    w_up,
    w_down,
    out_gate,
    in_gate,
    conv_input,
    conv_out,
    conv_taps,
    w_out,
):
    tok_rows = out_grad.shape[0]
    features = out_grad.shape[1]
    top_count = routes.shape[1]
    slices = lax.axis_size("sp")
    experts = slices // 2
    capacity = 5 * tok_rows // slices
    n_assign = tok_rows * top_count
    resid_f32 = residual.astype(jnp.float32)
    inv_rms = lax.rsqrt(jnp.mean(resid_f32 * resid_f32, axis=-1, keepdims=True) + epsilon)
    unit_rows = resid_f32 * inv_rms
    normed = unit_rows.astype(jnp.bfloat16)
    weighted = (
        (route_weights[:, :, None] * out_grad.astype(jnp.float32)[:, None, :])
        .astype(jnp.bfloat16)
        .reshape(n_assign, features)
    )
    flat_routes = routes.reshape(-1)
    onehot = (flat_routes[:, None] == jnp.arange(experts, dtype=jnp.int32)[None, :]).astype(
        jnp.int32
    )
    slot_rank = jnp.sum((jnp.cumsum(onehot, axis=0) - onehot) * onehot, axis=1)
    slot_index = flat_routes * capacity + slot_rank
    slot_table = (
        jnp.full((experts * capacity,), n_assign, jnp.int32)
        .at[slot_index]
        .set(jnp.arange(n_assign, dtype=jnp.int32))
    )
    filled = slot_table < n_assign
    safe_index = jnp.where(filled, slot_table, 0)
    send_rows = jnp.where(
        filled[:, None], normed[safe_index // top_count], jnp.zeros((), jnp.bfloat16)
    )
    send_grads = jnp.where(filled[:, None], weighted[safe_index], jnp.zeros((), jnp.bfloat16))
    outgoing = jnp.stack([send_rows, send_grads])
    doubled = jnp.repeat(outgoing.reshape(2, experts, capacity, features), 2, axis=1)
    arrived = lax.all_to_all(doubled, "sp", split_axis=1, concat_axis=1, tiled=True)
    expert_rows = arrived[0].reshape(slices * capacity, features)
    expert_grads = arrived[1].reshape(slices * capacity, features)
    gate_local = w_gate[0]
    up_local = w_up[0]
    down_local = w_down[0]
    pre_gate = jnp.dot(expert_rows, gate_local, preferred_element_type=jnp.float32)
    pre_up = jnp.dot(expert_rows, up_local, preferred_element_type=jnp.float32)
    sigmoid_gate = jax.nn.sigmoid(pre_gate)
    activated = pre_gate * sigmoid_gate
    hidden = (activated * pre_up).astype(jnp.bfloat16)
    d_hidden = lax.dot_general(
        expert_grads, down_local, (((1,), (1,)), ((), ())), preferred_element_type=jnp.float32
    )
    grad_down = lax.dot_general(
        hidden, expert_grads, (((0,), (0,)), ((), ())), preferred_element_type=jnp.float32
    ).astype(jnp.bfloat16)
    d_gate = (d_hidden * pre_up * sigmoid_gate * (1.0 + pre_gate * (1.0 - sigmoid_gate))).astype(
        jnp.bfloat16
    )
    d_up = (d_hidden * activated).astype(jnp.bfloat16)
    grad_up = lax.dot_general(
        expert_rows, d_up, (((0,), (0,)), ((), ())), preferred_element_type=jnp.float32
    ).astype(jnp.bfloat16)
    partial_value = lax.dot_general(
        d_gate, gate_local, (((1,), (1,)), ((), ())), preferred_element_type=jnp.float32
    )
    partial_value = partial_value + lax.dot_general(
        d_up, up_local, (((1,), (1,)), ((), ())), preferred_element_type=jnp.float32
    )
    partial_value = partial_value.astype(jnp.bfloat16).reshape(slices, capacity, features)
    summed = lax.psum_scatter(partial_value, "tp", scatter_dimension=2, tiled=True).astype(
        jnp.float32
    )
    returned = lax.all_to_all(
        summed.astype(jnp.bfloat16), "sp", split_axis=0, concat_axis=0, tiled=True
    )
    columns = returned.shape[2]
    flat_back = returned.reshape(slices * capacity, columns)
    first_index = 2 * flat_routes * capacity + slot_rank
    contrib = flat_back[first_index].astype(jnp.float32) + flat_back[first_index + capacity].astype(
        jnp.float32
    )
    d_normed = jnp.sum(contrib.reshape(tok_rows, top_count, columns), axis=1)
    col_start = lax.axis_index("tp") * columns
    unit_part = lax.dynamic_slice_in_dim(unit_rows, col_start, columns, 1)
    grad_part = lax.dynamic_slice_in_dim(out_grad, col_start, columns, 1).astype(jnp.float32)
    row_dots = lax.psum(jnp.sum(unit_part * d_normed, axis=-1), "tp")
    row_mean = row_dots[:, None] / features
    resid_part = (grad_part + inv_rms * (d_normed - unit_part * row_mean)).astype(jnp.bfloat16)
    grad_resid = lax.all_gather(resid_part, "tp", axis=1, tiled=True)
    d_mix = lax.dot_general(
        grad_resid, w_out, (((1,), (1,)), ((), ())), preferred_element_type=jnp.float32
    )
    conv_f32 = conv_out.astype(jnp.float32)
    gate_f32 = out_gate.astype(jnp.float32)
    grad_out_gate = (d_mix * conv_f32).astype(jnp.bfloat16)
    d_conv = d_mix * gate_f32
    padded = with_halo(d_conv.astype(jnp.bfloat16), (("sp", 0),), 1).astype(d_conv.dtype)
    d_inner = conv_taps[0] * padded[2:] + conv_taps[1] * padded[1:-1] + conv_taps[2] * padded[:-2]
    grad_in_gate = (d_inner * conv_input.astype(jnp.float32)).astype(jnp.bfloat16)
    grad_conv_input = (d_inner * in_gate.astype(jnp.float32)).astype(jnp.bfloat16)
    mixed = (gate_f32 * conv_f32).astype(jnp.bfloat16)
    grad_w_out = lax.psum_scatter(
        lax.dot_general(
            grad_resid, mixed, (((0,), (0,)), ((), ())), preferred_element_type=jnp.float32
        ),
        "sp",
        scatter_dimension=0,
        tiled=True,
    )
    return (
        grad_resid,
        grad_up[None],
        grad_down[None],
        grad_out_gate,
        grad_in_gate,
        grad_conv_input,
        grad_w_out,
    )


MESH = pl.DeviceIdType.MESH
BF16 = jnp.bfloat16
F32 = jnp.float32
VMEM_LIMIT = 60 * 1024 * 1024


def place():
    sp, tp = lax.axis_index("sp"), lax.axis_index("tp")
    return sp, tp, lax.div(sp, 2), lax.rem(sp, 2), lax.div(tp, 2), lax.rem(tp, 2)


def greet(peers):
    barrier = pltpu.get_barrier_semaphore()
    for peer in peers:
        pl.semaphore_signal(barrier, inc=1, device_id=peer, device_id_type=MESH)
    return lambda: pl.semaphore_wait(barrier, len(peers))


def columns_of(index, width):
    return pl.ds(pl.multiple_of(index * width, width), width)


def rows_of(index, height):
    return pl.ds(pl.multiple_of(index * height, height), height)


def layer_kernel(
    slices, cap,
    rt_hbm, rw_hbm, resid_hbm, og_hbm, gate_hbm, up_hbm, down_hbm,
    ogate_hbm, igate_hbm, cin_hbm, cout_hbm, taps_hbm, wout_hbm,
    gresid_hbm, gup_hbm, gdown_hbm, gogate_hbm, gigate_hbm, gcin_hbm, gwout_hbm,
    rt, rw, resid, og, gate, up, down, ogate, igate, cin, cout, taps, wout,
    gresid, gup, gdown, gogate, gigate, gcin, gwout,
    rows, grads, hidden, d_gate, d_up, sel, send_rows, send_grads,
    part, sib, pairsum, plane, zsend, ret, dn, edge_out, edge_in, grx, mixed,
    send_sem, recv_sem, in_sem, out_sem,
):
    sp, tp, z, y, x, c = place()
    pairs = slices // 2
    tok, features = resid.shape
    units = gate.shape[1]
    width = features // 4
    sibling = (sp, 2 * x + 1 - c)
    x_peer = (sp, 2 * (1 - x) + c)
    y_peer = (2 * z + 1 - y, tp)
    diagonal = (2 * z + 1 - y, 2 * (1 - x) + c)
    sp_peers = [(lax.rem(sp + k, slices), tp) for k in range(1, slices)]
    ready = greet(sp_peers + [sibling, x_peer, diagonal])

    def pair_of(k):
        pair, bit = 0, 1
        while bit < pairs:
            pair = pair + bit * lax.rem(lax.rem(lax.div(z, bit), 2) + (k // bit) % 2, 2)
            bit *= 2
        return pair

    def fetch(n, src, dst):
        copy = pltpu.make_async_copy(src, dst, in_sem.at[n])
        copy.start()
        return copy

    first = [
        fetch(n, src, dst)
        for n, (src, dst) in enumerate(
            ((resid_hbm, resid), (rt_hbm, rt), (rw_hbm, rw), (og_hbm, og))
        )
    ]
    weights = [
        fetch(4 + n, src, dst)
        for n, (src, dst) in enumerate(((gate_hbm, gate), (up_hbm, up), (down_hbm, down)))
    ]
    gates = [
        fetch(7 + n, src, dst)
        for n, (src, dst) in enumerate(
            (
                (ogate_hbm, ogate), (cout_hbm, cout), (wout_hbm, wout),
                (igate_hbm, igate), (cin_hbm, cin), (taps_hbm, taps),
            )
        )
    ]
    started, stored = [], []

    def send(src, dst, peer):
        n = len(started)
        copy = pltpu.make_async_remote_copy(
            src_ref=src, dst_ref=dst, send_sem=send_sem.at[n], recv_sem=recv_sem.at[n],
            device_id=peer, device_id_type=MESH,
        )
        copy.start()
        started.append(copy)
        return copy

    def store(src, dst):
        copy = pltpu.make_async_copy(src, dst, out_sem.at[len(stored)])
        copy.start()
        stored.append(copy)

    def block(pair, yy, xx, cc):
        return (rows_of(2 * pair + yy, cap), columns_of(2 * xx + cc, width))

    for copy in first:
        copy.wait()
    grid_r = lax.broadcasted_iota(jnp.int32, (tok, tok), 0)
    grid_c = lax.broadcasted_iota(jnp.int32, (tok, tok), 1)
    earlier = (grid_r < grid_c).astype(F32).astype(BF16)
    slot = lax.broadcasted_iota(jnp.int32, (cap, tok), 0).astype(F32)
    r32 = resid[...].astype(F32)
    inv_rms = lax.rsqrt(jnp.mean(r32 * r32, axis=-1, keepdims=True) + epsilon)
    mine = columns_of(tp, width)
    normed = (resid[:, mine].astype(F32) * inv_rms).astype(BF16)
    cot = og[:, mine]

    def choose(e):
        named = (rt[...] == e).astype(F32)
        mask = jnp.sum(named, axis=0, keepdims=True)
        weight = jnp.sum(named * rw[...], axis=0, keepdims=True)
        rank = jnp.dot(
            jnp.broadcast_to(mask, (8, tok)).astype(BF16), earlier, preferred_element_type=F32
        )[0:1]
        pick = jnp.where((rank == slot) & (mask > 0.5), 1.0, 0.0)
        slot_weight = jnp.sum(pick * weight, axis=1, keepdims=True)
        pick = pick.astype(BF16)
        sel[rows_of(e, cap), :] = pick
        return pick, slot_weight

    arriving = {}
    home = block(z, y, x, c)
    for k in range(1, pairs):
        e = pair_of(k)
        pick, slot_weight = choose(e)
        here = rows_of(e, cap)
        send_rows[here, :] = jnp.dot(pick, normed, preferred_element_type=F32).astype(BF16)
        send_grads[here, :] = (
            slot_weight * jnp.dot(pick, cot, preferred_element_type=F32)
        ).astype(BF16)
        if k == 1:
            ready()
        for a, (src, dst) in enumerate(((send_rows, rows), (send_grads, grads))):
            arriving[k, a] = send(src.at[here, :], dst.at[home], (2 * e + y, tp))
    pick, slot_weight = choose(z)
    own_rows = rows_of(sp, cap)
    rows[own_rows, :] = jnp.dot(
        pick, (r32 * inv_rms).astype(BF16), preferred_element_type=F32
    ).astype(BF16)
    grads[own_rows, :] = (
        slot_weight * jnp.dot(pick, og[...], preferred_element_type=F32)
    ).astype(BF16)

    both = (rows, grads)
    outs = [{} for _ in range(pairs)]

    def spread(k):
        out, at = outs[k], block(pair_of(k), y, x, c)
        if k == 0:
            for a, ref in enumerate(both):
                out["y", a] = send(ref.at[at], ref.at[at], y_peer)
            return
        for a, ref in enumerate(both):
            arriving[k, a].wait_recv()
            out["x", a] = send(ref.at[at], ref.at[at], x_peer)
            out["y", a] = send(ref.at[at], ref.at[at], y_peer)
            out["s", a] = send(ref.at[at], ref.at[at], sibling)

    def forward(k):
        out, pair = outs[k], pair_of(k)
        got_x = block(pair, y, 1 - x, c)
        got_y = block(pair, 1 - y, x, c)

        def pass_on(kind, got, a):
            out["s" + kind, a] = send(both[a].at[got], both[a].at[got], sibling)

        if k == 0:
            for a, ref in enumerate(both):
                out["y", a].wait_recv()
                out["d", a] = send(ref.at[got_y], ref.at[got_y], x_peer)
                pass_on("y", got_y, a)
            return
        out["x", 0].wait_recv()
        out["d", 0] = send(rows.at[got_x], rows.at[got_x], y_peer)
        pass_on("x", got_x, 0)
        out["y", 1].wait_recv()
        out["d", 1] = send(grads.at[got_y], grads.at[got_y], x_peer)
        pass_on("y", got_y, 1)
        out["x", 1].wait_recv()
        pass_on("x", got_x, 1)
        out["y", 0].wait_recv()
        pass_on("y", got_y, 0)

    def finish(k):
        out, got = outs[k], block(pair_of(k), 1 - y, 1 - x, c)
        for a, ref in enumerate(both):
            out["d", a].wait_recv()
            out["sd", a] = send(ref.at[got], ref.at[got], sibling)

    def experts(k):
        for kind in ("s", "sx", "sy", "sd"):
            for a in range(2):
                if (kind, a) in outs[k]:
                    outs[k][kind, a].wait_recv()
        at = rows_of(pair_of(k), 2 * cap)
        pre_gate = jnp.dot(rows[at, :], gate[...], preferred_element_type=F32)
        pre_up = jnp.dot(rows[at, :], up[...], preferred_element_type=F32)
        d_hidden = lax.dot_general(
            grads[at, :], down[...], (((1,), (1,)), ((), ())), preferred_element_type=F32
        )
        sigmoid_gate = jax.nn.sigmoid(pre_gate)
        activated = pre_gate * sigmoid_gate
        hidden[at, :] = (activated * pre_up).astype(BF16)
        d_gate[at, :] = (
            d_hidden * pre_up * sigmoid_gate * (1.0 + pre_gate * (1.0 - sigmoid_gate))
        ).astype(BF16)
        d_up[at, :] = (d_hidden * activated).astype(BF16)

    across_units = (((1,), (1,)), ((), ()))
    halves, moved, back = {}, {}, []

    def partials(k):
        at = rows_of(pair_of(k), 2 * cap)
        part[at, :] = (
            lax.dot_general(d_gate[at, :], gate[...], across_units, preferred_element_type=F32)
            + lax.dot_general(d_up[at, :], up[...], across_units, preferred_element_type=F32)
        ).astype(BF16)
        for h in range(2):
            halves[k, h] = send(
                part.at[at, columns_of(2 * h + 1 - c, width)], sib.at[h, at, :], sibling
            )

    def reduce_cores(k):
        pair = pair_of(k)
        at = rows_of(pair, 2 * cap)
        for h in range(2):
            halves[k, h].wait_recv()
            pairsum[h, at, :] = (
                part[at, columns_of(2 * h + c, width)].astype(F32) + sib[h, at, :].astype(F32)
            ).astype(BF16)
        same, other = rows_of(2 * pair + y, cap), rows_of(2 * pair + 1 - y, cap)
        slots = rows_of(pair, cap)
        moved[k] = [
            send(pairsum.at[1 - x, other, :], plane.at[2, slots, :], diagonal),
            send(pairsum.at[1 - x, same, :], plane.at[0, slots, :], x_peer),
            send(pairsum.at[x, other, :], plane.at[1, slots, :], y_peer),
        ]

    def reduce_plane(k):
        pair = pair_of(k)
        slots = rows_of(pair, cap)
        for copy in moved[k]:
            copy.wait_recv()
        total = (
            pairsum[x, rows_of(2 * pair + y, cap), :].astype(F32)
            + plane[0, slots, :].astype(F32)
            + plane[1, slots, :].astype(F32)
            + plane[2, slots, :].astype(F32)
        ).astype(BF16)
        if k:
            zsend[slots, :] = total
            back.append(
                send(zsend.at[slots, :], ret.at[rows_of(z, cap), :], (2 * pair + y, tp))
            )
        else:
            ret[slots, :] = total

    over_rows = (((0,), (0,)), ((), ()))

    def down_chunk(n):
        at = slice(n * units // 2, (n + 1) * units // 2)
        gdown[at, :] = lax.dot_general(
            hidden[:, at], grads[...], over_rows, preferred_element_type=F32
        ).astype(BF16)
        store(gdown.at[at, :], gdown_hbm.at[at, :])

    def up_chunk(n):
        at = slice(n * features // 4, (n + 1) * features // 4)
        gup[at, :] = lax.dot_general(
            rows[:, at], d_up[...], over_rows, preferred_element_type=F32
        ).astype(BF16)
        store(gup.at[at, :], gup_hbm.at[at, :])

    own = rows_of(sp, tok)

    def share_mixed():
        for copy in gates:
            copy.wait()
        mixed[own, :] = (ogate[...].astype(F32) * cout[...].astype(F32)).astype(BF16)
        return [send(mixed.at[own, :], mixed.at[own, :], peer) for peer in sp_peers]

    spread(0)
    forward(0)
    spread(1)
    finish(0)
    forward(1)
    for copy in weights:
        copy.wait()
    experts(0)
    spread(2)
    finish(1)
    partials(0)
    forward(2)
    experts(1)
    for k in range(3, pairs):
        spread(k)
        finish(k - 1)
        partials(k - 2)
        forward(k)
        if k == pairs - 1:
            mixed_copies = share_mixed()
        experts(k - 1)
    finish(pairs - 1)
    reduce_cores(1)
    partials(pairs - 2)
    for k in range(2, pairs - 1):
        reduce_cores(k)
    experts(pairs - 1)
    partials(pairs - 1)
    reduce_plane(1)
    down_chunk(0)
    reduce_cores(pairs - 1)
    reduce_cores(0)
    down_chunk(1)
    for k in range(2, pairs - 1):
        reduce_plane(k)
    up_chunk(0)
    up_chunk(1)
    reduce_plane(pairs - 1)
    reduce_plane(0)
    up_chunk(2)
    up_chunk(3)

    for copy in back:
        copy.wait_recv()
    dn[:, mine] = lax.dot_general(
        sel[...], ret[...], over_rows, preferred_element_type=F32
    ).astype(BF16)
    half = tok // 2
    far = columns_of(2 * (1 - x) + c, width)
    shares, relays = [], []
    for h in range(2):
        at = slice(h * half, (h + 1) * half)
        shares.append(send(dn.at[at, mine], dn.at[at, mine], x_peer))
    near = send(dn.at[:, mine], dn.at[:, mine], sibling)
    for h in range(2):
        at = slice(h * half, (h + 1) * half)
        shares[h].wait_recv()
        relays.append(send(dn.at[at, far], dn.at[at, far], sibling))
    for copy in [near] + relays:
        copy.wait_recv()
    unit = r32 * inv_rms
    d_normed = dn[...].astype(F32)
    row_mean = jnp.mean(unit * d_normed, axis=-1, keepdims=True)
    gresid[...] = (og[...].astype(F32) + inv_rms * (d_normed - unit * row_mean)).astype(BF16)
    share = features // slices
    across = [
        send(
            gresid.at[rows_of(c, half), columns_of(peer[0], share)],
            grx.at[rows_of(2 * sp + c, half), :], peer,
        )
        for peer in sp_peers
    ]
    store(gresid, gresid_hbm)
    d_mix = lax.dot_general(
        gresid[...], wout[...], (((1,), (1,)), ((), ())), preferred_element_type=F32
    )
    d_conv = d_mix * ogate[...].astype(F32)
    edge_out[0] = d_conv[tok - 8 :]
    edge_out[1] = d_conv[:8]
    edges = [
        send(edge_out.at[0], edge_in.at[0], sp_peers[0]),
        send(edge_out.at[1], edge_in.at[1], sp_peers[-1]),
    ]
    gogate[...] = (d_mix * cout[...].astype(F32)).astype(BF16)
    store(gogate, gogate_hbm)
    grx[own, :] = gresid[:, columns_of(sp, share)]
    passed = []
    for n in range(slices - 1):
        across[n].wait_recv()
        got = grx.at[rows_of(2 * lax.rem(sp + slices - 1 - n, slices) + c, half), :]
        passed.append(send(got, got, sibling))
    for copy in edges:
        copy.wait_recv()
    before = jnp.where(sp > 0, edge_in[0, 7:8, :], 0.0)
    after = jnp.where(sp < slices - 1, edge_in[1, 0:1, :], 0.0)
    at = lax.broadcasted_iota(jnp.int32, d_conv.shape, 0)
    later = jnp.where(at == tok - 1, after, pltpu.roll(d_conv, tok - 1, 0))
    former = jnp.where(at == 0, before, pltpu.roll(d_conv, 1, 0))
    d_inner = taps[0:1, :] * later + taps[1:2, :] * d_conv + taps[2:3, :] * former
    gigate[...] = (d_inner * cin[...].astype(F32)).astype(BF16)
    store(gigate, gigate_hbm)
    gcin[...] = (d_inner * igate[...].astype(F32)).astype(BF16)
    store(gcin, gcin_hbm)
    for copy in passed + mixed_copies:
        copy.wait_recv()
    gwout[...] = lax.dot_general(grx[...], mixed[...], over_rows, preferred_element_type=F32)
    store(gwout, gwout_hbm)
    for copy in started:
        copy.wait_send()
    for copy in stored:
        copy.wait()


def layer(slices, cap, args):
    rt, rw, resid, og, gate, up, down, ogate, igate, cin, cout, taps, wout = args
    tok, features = resid.shape
    units, channels = gate.shape[1], ogate.shape[1]
    pairs, width = slices // 2, features // 4
    anywhere = pl.BlockSpec(memory_space=pl.ANY)
    share = features // slices
    outs = (
        (resid.shape, BF16), (gate.shape, BF16), (down.shape, BF16),
        (ogate.shape, BF16), (ogate.shape, BF16), (ogate.shape, BF16), ((share, channels), F32),
    )
    rows = slices * cap
    sems = 26 * pairs + 3 * slices + 8
    return pl.pallas_call(
        functools.partial(layer_kernel, slices, cap),
        out_shape=tuple(jax.ShapeDtypeStruct(*out) for out in outs),
        in_specs=[anywhere] * len(args),
        out_specs=[anywhere] * len(outs),
        scratch_shapes=[pltpu.VMEM(arg.shape, arg.dtype) for arg in args]
        + [pltpu.VMEM(*out) for out in outs]
        + [
            pltpu.VMEM((rows, features), BF16),
            pltpu.VMEM((rows, features), BF16),
            pltpu.VMEM((rows, units), BF16),
            pltpu.VMEM((rows, units), BF16),
            pltpu.VMEM((rows, units), BF16),
            pltpu.VMEM((pairs * cap, tok), BF16),
            pltpu.VMEM((pairs * cap, width), BF16),
            pltpu.VMEM((pairs * cap, width), BF16),
            pltpu.VMEM((rows, features), BF16),
            pltpu.VMEM((2, rows, width), BF16),
            pltpu.VMEM((2, rows, width), BF16),
            pltpu.VMEM((3, pairs * cap, width), BF16),
            pltpu.VMEM((pairs * cap, width), BF16),
            pltpu.VMEM((pairs * cap, width), BF16),
            pltpu.VMEM((tok, features), BF16),
            pltpu.VMEM((2, 8, channels), F32),
            pltpu.VMEM((2, 8, channels), F32),
            pltpu.VMEM((slices * tok, share), BF16),
            pltpu.VMEM((slices * tok, channels), BF16),
            pltpu.SemaphoreType.DMA((sems,)),
            pltpu.SemaphoreType.DMA((sems,)),
            pltpu.SemaphoreType.DMA((len(args),)),
            pltpu.SemaphoreType.DMA((len(outs) + 4,)),
        ],
        compiler_params=pltpu.CompilerParams(
            collective_id=0, has_side_effects=True, vmem_limit_bytes=VMEM_LIMIT
        ),
        name="layer",
    )(*args)


def publish_kernel(count, chunks, *refs):
    srcs, dsts, held = refs[:count], refs[count : 2 * count], refs[2 * count : 3 * count]
    in_sem, out_sem = refs[3 * count :]
    pieces = []
    for src, dst, buf, cut in zip(srcs, dsts, held, chunks):
        height = src.shape[0] // cut
        for n in range(cut):
            at = pl.ds(n * height, height)
            i = len(pieces)
            pieces.append(
                (
                    pltpu.make_async_copy(src.at[at, :], buf.at[at, :], in_sem.at[i]),
                    pltpu.make_async_copy(buf.at[at, :], dst.at[at, :], out_sem.at[i]),
                )
            )
    for take, _ in pieces:
        take.start()
    for take, give in pieces:
        take.wait()
        give.start()
    for _, give in pieces:
        give.wait()


def publish(arrays):
    chunks = [max(1, a.size * a.dtype.itemsize // (512 * 1024)) for a in arrays]
    anywhere = pl.BlockSpec(memory_space=pl.ANY)
    return pl.pallas_call(
        functools.partial(publish_kernel, len(arrays), chunks),
        out_shape=tuple(jax.ShapeDtypeStruct(a.shape, a.dtype) for a in arrays),
        in_specs=[anywhere] * len(arrays),
        out_specs=[anywhere] * len(arrays),
        scratch_shapes=[pltpu.VMEM(a.shape, a.dtype) for a in arrays]
        + [pltpu.SemaphoreType.DMA((sum(chunks),))] * 2,
        compiler_params=pltpu.CompilerParams(vmem_limit_bytes=VMEM_LIMIT),
        name="publish",
    )(*arrays)


def per_device(
    out_grad, residual, routes, route_weights, w_gate, w_up, w_down,
    out_gate, in_gate, conv_input, conv_out, conv_taps, w_out,
):
    slices = lax.axis_size("sp")
    cap = 5 * out_grad.shape[0] // slices
    results = layer(
        slices, cap,
        (
            routes.T, route_weights.T, residual, out_grad, w_gate[0], w_up[0], w_down[0],
            out_gate, in_gate, conv_input, conv_out, conv_taps, w_out,
        ),
    )
    grad_resid, grad_up, grad_down, *small = publish(results)
    return (grad_resid, grad_up[None], grad_down[None], *small)


def fits_kernels(mesh, tokens):
    slices = mesh.shape["sp"]
    rows = tokens // slices
    powers = slices >= 8 and slices & (slices - 1) == 0
    return mesh.shape["tp"] == 4 and powers and (5 * rows // slices) % 16 == 0


def on_device(mesh, out_grad, *rest):
    tokens = out_grad.shape[0] * mesh.shape["sp"]
    body = per_device if fits_kernels(mesh, tokens) else per_device_general
    return body(out_grad, *rest)


def solution(mesh):
    in_specs = (
        P("sp", None),
        P("sp", None),
        P("sp", None),
        P("sp", None),
        P("sp", None, "tp"),
        P("sp", None, "tp"),
        P("sp", "tp", None),
        P("sp", "tp"),
        P("sp", "tp"),
        P("sp", "tp"),
        P("sp", "tp"),
        P(None, "tp"),
        P("tp", None),
    )
    out_specs = (
        P("sp", None),
        P("sp", None, "tp"),
        P("sp", "tp", None),
        P("sp", "tp"),
        P("sp", "tp"),
        P("sp", "tp"),
        P("sp", "tp"),
    )
    return jax.shard_map(
        functools.partial(on_device, mesh), mesh=mesh, in_specs=in_specs, out_specs=out_specs, check_vma=False
    )
```

time: 98.6 us -> 80 us (0.81)
  Pallas kernels: 91.4 us -> 79.3 us
  matrix products: 6.32 us -> 0 us
    pallas_call x3 -> x2, Pallas kernels: 91.4 us -> 79.3 us  [the longest x1 74.7 us: layer(): pl.pallas_call(functools.partial(layer_kernel, slices, cap), out_shape=tu...]
    dot_general x2 -> x0, matrix products: 6.32 us -> none  [the longest x1 3.17 us: per_device(): lax.dot_general(hidden, expert_grads, (((0,), (0,)), ((), ())), preferred...]
where the time goes in v1:
time: 80 us; the launch traced here: 79.9 us
  Pallas kernels  79.3 us (99%)
    pallas_call x1, Pallas kernels, layer(): pl.pallas_call(functools.partial(layer_kernel, slices, cap), out_shape=tu...  74.7 us
    pallas_call x1, Pallas kernels, publish(): pl.pallas_call(functools.partial(publish_kernel, len(arrays), chunks), ou...  4.59 us

profile of v1, /device:TPU:0, one launch (start us, length us, event | category | flops | bytes accessed | tf_op | source)
XLA Modules:
  0.0 79.9 jit_solution(8194159134810427341)
XLA Ops:
  0.6 74.7 %layer.1 = (bf16[128,2048]{1,0:T(8,128)(2,1)}, bf16[2048,512]{1,0:T(8,128)(2,1)}, bf16[512,2048]{1,0:T(8,128)(2,1)}, bf16[128,256]{1,0:T(8,128)(2,1)}, bf16[128,...) custom-call(s32[2,128]{1,0:T(2,128)} %bitcast.10, f32[2,128]{1,0:T(2,128)} %bitcast.11, ...), custom_call_target="tpu_custom_call" | custom-call | tf_op jit(solution)/shard_map/layer/pallas_call | solution.py:574
  75.3 4.6 %publish.1 = (bf16[128,2048]{1,0:T(8,128)(2,1)}, bf16[2048,512]{1,0:T(8,128)(2,1)}, bf16[512,2048]{1,0:T(8,128)(2,1)}, bf16[128,256]{1,0:T(8,128)(2,1)}, bf16[12...) custom-call(bf16[128,2048]{1,0:T(8,128)(2,1)} %get-tuple-element.21.refs_0_, ...), custom_call_target="tpu_custom_call" | custom-call | tf_op jit(solution)/shard_map/publish/pallas_call | solution.py:640

commit v2 on v1

--- a/solution.py
+++ b/solution.py
@@ -1,4 +1,5 @@
 import functools
+import math
 
 import jax
 import jax.numpy as jnp
@@ -239,17 +240,37 @@
             )
         )
     ]
-    started, stored = [], []
-
-    def send(src, dst, peer):
-        n = len(started)
-        copy = pltpu.make_async_remote_copy(
-            src_ref=src, dst_ref=dst, send_sem=send_sem.at[n], recv_sem=recv_sem.at[n],
-            device_id=peer, device_id_type=MESH,
-        )
-        copy.start()
-        started.append(copy)
-        return copy
+    stored, unit_cols = [], gate.shape[1]
+    slots_used, leaving = [0], [[]]
+
+    def units_of(ref):
+        return math.prod(ref.shape) * jnp.dtype(ref.dtype).itemsize // (2 * unit_cols)
+
+    def await_units(sem, units):
+        assert units <= gate.shape[0]
+        like = gate.at[pl.ds(0, units), :]
+        pltpu.make_async_copy(like, like, sem).wait()
+
+    class Batch:
+        def __init__(self):
+            self.slot, self.units = slots_used[0], 0
+            slots_used[0] += 1
+
+        def wait_recv(self):
+            await_units(recv_sem.at[self.slot], self.units)
+
+    def send(src, dst, peer, batch=None):
+        batch = batch or Batch()
+        units = units_of(src)
+        batch.units += units
+        if sum(leaving[-1]) + units > gate.shape[0]:
+            leaving.append([])
+        leaving[-1].append(units)
+        pltpu.make_async_remote_copy(
+            src_ref=src, dst_ref=dst, send_sem=send_sem.at[len(leaving) - 1],
+            recv_sem=recv_sem.at[batch.slot], device_id=peer, device_id_type=MESH,
+        ).start()
+        return batch
 
     def store(src, dst):
         copy = pltpu.make_async_copy(src, dst, out_sem.at[len(stored)])
@@ -309,82 +330,71 @@
 
     both = (rows, grads)
     outs = [{} for _ in range(pairs)]
-
-    def spread(k):
-        out, at = outs[k], block(pair_of(k), y, x, c)
-        if k == 0:
-            for a, ref in enumerate(both):
-                out["y", a] = send(ref.at[at], ref.at[at], y_peer)
-            return
-        for a, ref in enumerate(both):
+    near_rows = [Batch() for _ in range(pairs)]
+
+    def spread(k, a):
+        out, ref, at = outs[k], both[a], block(pair_of(k), y, x, c)
+        if k:
             arriving[k, a].wait_recv()
             out["x", a] = send(ref.at[at], ref.at[at], x_peer)
-            out["y", a] = send(ref.at[at], ref.at[at], y_peer)
-            out["s", a] = send(ref.at[at], ref.at[at], sibling)
-
-    def forward(k):
-        out, pair = outs[k], pair_of(k)
-        got_x = block(pair, y, 1 - x, c)
-        got_y = block(pair, 1 - y, x, c)
-
-        def pass_on(kind, got, a):
-            out["s" + kind, a] = send(both[a].at[got], both[a].at[got], sibling)
-
-        if k == 0:
-            for a, ref in enumerate(both):
-                out["y", a].wait_recv()
-                out["d", a] = send(ref.at[got_y], ref.at[got_y], x_peer)
-                pass_on("y", got_y, a)
-            return
-        out["x", 0].wait_recv()
-        out["d", 0] = send(rows.at[got_x], rows.at[got_x], y_peer)
-        pass_on("x", got_x, 0)
-        out["y", 1].wait_recv()
-        out["d", 1] = send(grads.at[got_y], grads.at[got_y], x_peer)
-        pass_on("y", got_y, 1)
-        out["x", 1].wait_recv()
-        pass_on("x", got_x, 1)
-        out["y", 0].wait_recv()
-        pass_on("y", got_y, 0)
-
-    def finish(k):
-        out, got = outs[k], block(pair_of(k), 1 - y, 1 - x, c)
-        for a, ref in enumerate(both):
-            out["d", a].wait_recv()
-            out["sd", a] = send(ref.at[got], ref.at[got], sibling)
-
-    def experts(k):
-        for kind in ("s", "sx", "sy", "sd"):
-            for a in range(2):
-                if (kind, a) in outs[k]:
-                    outs[k][kind, a].wait_recv()
+        out["y", a] = send(ref.at[at], ref.at[at], y_peer)
+        if k:
+            send(ref.at[at], ref.at[at], sibling, near_rows[k])
+
+    def got_x(k, a):
+        out, ref, at = outs[k], both[a], block(pair_of(k), y, 1 - x, c)
+        out["x", a].wait_recv()
+        if a == 0:
+            out["d", a] = send(ref.at[at], ref.at[at], y_peer)
+        send(ref.at[at], ref.at[at], sibling, near_rows[k])
+
+    def got_y(k, a):
+        out, ref, at = outs[k], both[a], block(pair_of(k), 1 - y, x, c)
+        out["y", a].wait_recv()
+        if k == 0 or a == 1:
+            out["d", a] = send(ref.at[at], ref.at[at], x_peer)
+        send(ref.at[at], ref.at[at], sibling, near_rows[k])
+
+    def got_d(k, a):
+        out, ref, at = outs[k], both[a], block(pair_of(k), 1 - y, 1 - x, c)
+        out["d", a].wait_recv()
+        send(ref.at[at], ref.at[at], sibling, near_rows[k])
+
+    across_units = (((1,), (1,)), ((), ()))
+    held, halves, moved, back = {}, {}, {}, Batch()
+
+    def experts(k, step):
         at = rows_of(pair_of(k), 2 * cap)
-        pre_gate = jnp.dot(rows[at, :], gate[...], preferred_element_type=F32)
-        pre_up = jnp.dot(rows[at, :], up[...], preferred_element_type=F32)
-        d_hidden = lax.dot_general(
-            grads[at, :], down[...], (((1,), (1,)), ((), ())), preferred_element_type=F32
+        if step == 0:
+            near_rows[k].wait_recv()
+            held["gate"] = jnp.dot(rows[at, :], gate[...], preferred_element_type=F32)
+        elif step == 1:
+            held["up"] = jnp.dot(rows[at, :], up[...], preferred_element_type=F32)
+        else:
+            pre_gate, pre_up = held["gate"], held["up"]
+            d_hidden = lax.dot_general(
+                grads[at, :], down[...], across_units, preferred_element_type=F32
+            )
+            sigmoid_gate = jax.nn.sigmoid(pre_gate)
+            activated = pre_gate * sigmoid_gate
+            hidden[at, :] = (activated * pre_up).astype(BF16)
+            d_gate[at, :] = (
+                d_hidden * pre_up * sigmoid_gate * (1.0 + pre_gate * (1.0 - sigmoid_gate))
+            ).astype(BF16)
+            d_up[at, :] = (d_hidden * activated).astype(BF16)
+
+    def partials(k, h):
+        at = rows_of(pair_of(k), 2 * cap)
+        cols = slice(2 * h * width, 2 * (h + 1) * width)
+        part[at, cols] = (
+            lax.dot_general(
+                d_gate[at, :], gate[cols, :], across_units, preferred_element_type=F32
+            )
+            + lax.dot_general(d_up[at, :], up[cols, :], across_units, preferred_element_type=F32)
+        ).astype(BF16)
+        halves[k, h] = send(
+            part.at[at, columns_of(2 * h + 1 - c, width)], sib.at[h, at, :], sibling
         )
-        sigmoid_gate = jax.nn.sigmoid(pre_gate)
-        activated = pre_gate * sigmoid_gate
-        hidden[at, :] = (activated * pre_up).astype(BF16)
-        d_gate[at, :] = (
-            d_hidden * pre_up * sigmoid_gate * (1.0 + pre_gate * (1.0 - sigmoid_gate))
-        ).astype(BF16)
-        d_up[at, :] = (d_hidden * activated).astype(BF16)
-
-    across_units = (((1,), (1,)), ((), ()))
-    halves, moved, back = {}, {}, []
-
-    def partials(k):
-        at = rows_of(pair_of(k), 2 * cap)
-        part[at, :] = (
-            lax.dot_general(d_gate[at, :], gate[...], across_units, preferred_element_type=F32)
-            + lax.dot_general(d_up[at, :], up[...], across_units, preferred_element_type=F32)
-        ).astype(BF16)
-        for h in range(2):
-            halves[k, h] = send(
-                part.at[at, columns_of(2 * h + 1 - c, width)], sib.at[h, at, :], sibling
-            )
 
     def reduce_cores(k):
         pair = pair_of(k)
@@ -396,17 +406,18 @@
             ).astype(BF16)
         same, other = rows_of(2 * pair + y, cap), rows_of(2 * pair + 1 - y, cap)
         slots = rows_of(pair, cap)
-        moved[k] = [
-            send(pairsum.at[1 - x, other, :], plane.at[2, slots, :], diagonal),
-            send(pairsum.at[1 - x, same, :], plane.at[0, slots, :], x_peer),
-            send(pairsum.at[x, other, :], plane.at[1, slots, :], y_peer),
-        ]
+        moved[k] = Batch()
+        for n, src, peer in (
+            (2, pairsum.at[1 - x, other, :], diagonal),
+            (0, pairsum.at[1 - x, same, :], x_peer),
+            (1, pairsum.at[x, other, :], y_peer),
+        ):
+            send(src, plane.at[n, slots, :], peer, moved[k])
 
     def reduce_plane(k):
         pair = pair_of(k)
         slots = rows_of(pair, cap)
-        for copy in moved[k]:
-            copy.wait_recv()
+        moved[k].wait_recv()
         total = (
             pairsum[x, rows_of(2 * pair + y, cap), :].astype(F32)
             + plane[0, slots, :].astype(F32)
@@ -415,9 +426,7 @@
         ).astype(BF16)
         if k:
             zsend[slots, :] = total
-            back.append(
-                send(zsend.at[slots, :], ret.at[rows_of(z, cap), :], (2 * pair + y, tp))
-            )
+            send(zsend.at[slots, :], ret.at[rows_of(z, cap), :], (2 * pair + y, tp), back)
         else:
             ret[slots, :] = total
 
@@ -439,40 +448,62 @@
 
     own = rows_of(sp, tok)
 
+    mixed_z, mixed_y = Batch(), Batch()
+
     def share_mixed():
         for copy in gates:
             copy.wait()
         mixed[own, :] = (ogate[...].astype(F32) * cout[...].astype(F32)).astype(BF16)
-        return [send(mixed.at[own, :], mixed.at[own, :], peer) for peer in sp_peers]
-
-    spread(0)
-    forward(0)
-    spread(1)
-    finish(0)
-    forward(1)
+        for k in range(1, pairs):
+            peer = (2 * pair_of(k) + y, tp)
+            send(mixed.at[own, :], mixed.at[own, :], peer, mixed_z)
+
+    def relay_mixed():
+        mixed_z.wait_recv()
+        for k in range(pairs):
+            at = rows_of(2 * pair_of(k) + y, tok)
+            send(mixed.at[at, :], mixed.at[at, :], y_peer, mixed_y)
+
+    for a in range(2):
+        spread(0, a)
+    for a in range(2):
+        got_y(0, a)
+        spread(1, a)
     for copy in weights:
         copy.wait()
-    experts(0)
-    spread(2)
-    finish(1)
-    partials(0)
-    forward(2)
-    experts(1)
-    for k in range(3, pairs):
-        spread(k)
-        finish(k - 1)
-        partials(k - 2)
-        forward(k)
-        if k == pairs - 1:
-            mixed_copies = share_mixed()
-        experts(k - 1)
-    finish(pairs - 1)
-    reduce_cores(1)
-    partials(pairs - 2)
-    for k in range(2, pairs - 1):
+    for k in range(1, pairs):
+        if k == 1:
+            got_d(0, 0)
+        got_y(k, 0)
+        if k == 1:
+            got_x(k, 0)
+            got_y(k, 1)
+            got_d(0, 1)
+        if k + 1 < pairs:
+            spread(k + 1, 0)
+        experts(k - 1, 0)
+        if k > 1:
+            got_y(k, 1)
+            got_x(k, 0)
+        elif k + 1 < pairs:
+            spread(k + 1, 1)
+        experts(k - 1, 1)
+        if 1 < k < pairs - 1:
+            spread(k + 1, 1)
+        got_x(k, 1)
+        if k + 2 == pairs:
+            share_mixed()
+        experts(k - 1, 2)
+        partials(k - 1, 0)
+        got_d(k, 0)
+        got_d(k, 1)
+        partials(k - 1, 1)
+    for k in range(1, pairs - 1):
         reduce_cores(k)
-    experts(pairs - 1)
-    partials(pairs - 1)
+    for step in range(3):
+        experts(pairs - 1, step)
+    for h in range(2):
+        partials(pairs - 1, h)
     reduce_plane(1)
     down_chunk(0)
     reduce_cores(pairs - 1)
@@ -484,39 +515,47 @@
     up_chunk(1)
     reduce_plane(pairs - 1)
     reduce_plane(0)
-    up_chunk(2)
-    up_chunk(3)
-
-    for copy in back:
-        copy.wait_recv()
+    relay_mixed()
+
+    back.wait_recv()
     dn[:, mine] = lax.dot_general(
         sel[...], ret[...], over_rows, preferred_element_type=F32
     ).astype(BF16)
-    half = tok // 2
+    half, quarter = tok // 2, tok // 4
     far = columns_of(2 * (1 - x) + c, width)
-    shares, relays = [], []
-    for h in range(2):
-        at = slice(h * half, (h + 1) * half)
-        shares.append(send(dn.at[at, mine], dn.at[at, mine], x_peer))
-    near = send(dn.at[:, mine], dn.at[:, mine], sibling)
-    for h in range(2):
-        at = slice(h * half, (h + 1) * half)
+    tops = [slice(h * half, (h + 1) * half) for h in range(2)]
+    shares = [send(dn.at[at, mine], dn.at[at, mine], x_peer) for at in tops]
+    near = [send(dn.at[at, mine], dn.at[at, mine], sibling) for at in tops]
+    share = features // slices
+    across = []
+
+    def share_rows(h):
         shares[h].wait_recv()
-        relays.append(send(dn.at[at, far], dn.at[at, far], sibling))
-    for copy in [near] + relays:
-        copy.wait_recv()
-    unit = r32 * inv_rms
-    d_normed = dn[...].astype(F32)
-    row_mean = jnp.mean(unit * d_normed, axis=-1, keepdims=True)
-    gresid[...] = (og[...].astype(F32) + inv_rms * (d_normed - unit * row_mean)).astype(BF16)
-    share = features // slices
-    across = [
-        send(
-            gresid.at[rows_of(c, half), columns_of(peer[0], share)],
-            grx.at[rows_of(2 * sp + c, half), :], peer,
-        )
-        for peer in sp_peers
-    ]
+        send(dn.at[tops[h], far], dn.at[tops[h], far], sibling, near[h])
+        if h == 0:
+            up_chunk(2)
+        near[h].wait_recv()
+
+    def resid_rows(h):
+        at = tops[h]
+        unit = r32[at] * inv_rms[at]
+        d_normed = dn[at, :].astype(F32)
+        row_mean = jnp.mean(unit * d_normed, axis=-1, keepdims=True)
+        gresid[at, :] = (
+            og[at, :].astype(F32) + inv_rms[at] * (d_normed - unit * row_mean)
+        ).astype(BF16)
+        for peer in sp_peers:
+            across.append(
+                send(
+                    gresid.at[rows_of(2 * h + c, quarter), columns_of(peer[0], share)],
+                    grx.at[rows_of(4 * sp + 2 * h + c, quarter), :], peer,
+                )
+            )
+
+    share_rows(0)
+    resid_rows(0)
+    share_rows(1)
+    resid_rows(1)
     store(gresid, gresid_hbm)
     d_mix = lax.dot_general(
         gresid[...], wout[...], (((1,), (1,)), ((), ())), preferred_element_type=F32
@@ -524,20 +563,20 @@
     d_conv = d_mix * ogate[...].astype(F32)
     edge_out[0] = d_conv[tok - 8 :]
     edge_out[1] = d_conv[:8]
-    edges = [
-        send(edge_out.at[0], edge_in.at[0], sp_peers[0]),
-        send(edge_out.at[1], edge_in.at[1], sp_peers[-1]),
-    ]
+    edges, passed = Batch(), Batch()
+    send(edge_out.at[0], edge_in.at[0], sp_peers[0], edges)
+    send(edge_out.at[1], edge_in.at[1], sp_peers[-1], edges)
     gogate[...] = (d_mix * cout[...].astype(F32)).astype(BF16)
     store(gogate, gogate_hbm)
     grx[own, :] = gresid[:, columns_of(sp, share)]
-    passed = []
-    for n in range(slices - 1):
-        across[n].wait_recv()
-        got = grx.at[rows_of(2 * lax.rem(sp + slices - 1 - n, slices) + c, half), :]
-        passed.append(send(got, got, sibling))
-    for copy in edges:
-        copy.wait_recv()
+    up_chunk(3)
+    for h in range(2):
+        for n in range(slices - 1):
+            across[h * (slices - 1) + n].wait_recv()
+            origin = lax.rem(sp + slices - 1 - n, slices)
+            got = grx.at[rows_of(4 * origin + 2 * h + c, quarter), :]
+            send(got, got, sibling, passed)
+    edges.wait_recv()
     before = jnp.where(sp > 0, edge_in[0, 7:8, :], 0.0)
     after = jnp.where(sp < slices - 1, edge_in[1, 0:1, :], 0.0)
     at = lax.broadcasted_iota(jnp.int32, d_conv.shape, 0)
@@ -548,14 +587,15 @@
     store(gigate, gigate_hbm)
     gcin[...] = (d_inner * igate[...].astype(F32)).astype(BF16)
     store(gcin, gcin_hbm)
-    for copy in passed + mixed_copies:
-        copy.wait_recv()
+    passed.wait_recv()
+    mixed_y.wait_recv()
     gwout[...] = lax.dot_general(grx[...], mixed[...], over_rows, preferred_element_type=F32)
     store(gwout, gwout_hbm)
-    for copy in started:
-        copy.wait_send()
+    for n, units in enumerate(leaving):
+        await_units(send_sem.at[n], sum(units))
     for copy in stored:
         copy.wait()
+    assert slots_used[0] == recv_sem.shape[0] and len(leaving) <= send_sem.shape[0]
 
 
 def layer(slices, cap, args):
@@ -570,7 +610,7 @@
         (ogate.shape, BF16), (ogate.shape, BF16), (ogate.shape, BF16), ((share, channels), F32),
     )
     rows = slices * cap
-    sems = 26 * pairs + 3 * slices + 8
+    sems = 12 * pairs + 2 * slices + 3
     return pl.pallas_call(
         functools.partial(layer_kernel, slices, cap),
         out_shape=tuple(jax.ShapeDtypeStruct(*out) for out in outs),
@@ -598,7 +638,7 @@
             pltpu.VMEM((2, 8, channels), F32),
             pltpu.VMEM((slices * tok, share), BF16),
             pltpu.VMEM((slices * tok, channels), BF16),
-            pltpu.SemaphoreType.DMA((sems,)),
+            pltpu.SemaphoreType.DMA((5,)),
             pltpu.SemaphoreType.DMA((sems,)),
             pltpu.SemaphoreType.DMA((len(args),)),
             pltpu.SemaphoreType.DMA((len(outs) + 4,)),

time: 80 us -> 73.9 us (0.924)
  Pallas kernels: 79.3 us -> 73.1 us
    pallas_call x1, Pallas kernels: 74.7 us -> 68.5 us  [layer(): pl.pallas_call(functools.partial(layer_kernel, slices, cap), out_shape=tu...]
where the time goes in v2:
time: 73.9 us; the launch traced here: 73.7 us
  Pallas kernels  73.1 us (99%)
    pallas_call x1, Pallas kernels, layer(): pl.pallas_call(functools.partial(layer_kernel, slices, cap), out_shape=tu...  68.5 us
    pallas_call x1, Pallas kernels, publish(): pl.pallas_call(functools.partial(publish_kernel, len(arrays), chunks), ou...  4.59 us

profile of v2, /device:TPU:0, one launch (start us, length us, event | category | flops | bytes accessed | tf_op | source)
XLA Modules:
  0.0 73.7 jit_solution(529680040959582102)
XLA Ops:
  0.6 68.5 %layer.1 = (bf16[128,2048]{1,0:T(8,128)(2,1)}, bf16[2048,512]{1,0:T(8,128)(2,1)}, bf16[512,2048]{1,0:T(8,128)(2,1)}, bf16[128,256]{1,0:T(8,128)(2,1)}, bf16[128,...) custom-call(s32[2,128]{1,0:T(2,128)} %bitcast.10, f32[2,128]{1,0:T(2,128)} %bitcast.11, ...), custom_call_target="tpu_custom_call" | custom-call | tf_op jit(solution)/shard_map/layer/pallas_call | solution.py:614
  69.1 4.6 %publish.1 = (bf16[128,2048]{1,0:T(8,128)(2,1)}, bf16[2048,512]{1,0:T(8,128)(2,1)}, bf16[512,2048]{1,0:T(8,128)(2,1)}, bf16[128,256]{1,0:T(8,128)(2,1)}, bf16[12...) custom-call(bf16[128,2048]{1,0:T(8,128)(2,1)} %get-tuple-element.21.refs_0_, ...), custom_call_target="tpu_custom_call" | custom-call | tf_op jit(solution)/shard_map/publish/pallas_call | solution.py:680

commit v3 on v2

--- a/solution.py
+++ b/solution.py
@@ -190,12 +190,11 @@
     slices, cap,
     rt_hbm, rw_hbm, resid_hbm, og_hbm, gate_hbm, up_hbm, down_hbm,
     ogate_hbm, igate_hbm, cin_hbm, cout_hbm, taps_hbm, wout_hbm,
-    gresid_hbm, gup_hbm, gdown_hbm, gogate_hbm, gigate_hbm, gcin_hbm, gwout_hbm,
+    gresid, gup, gdown, gogate, gigate, gcin, gwout,
     rt, rw, resid, og, gate, up, down, ogate, igate, cin, cout, taps, wout,
-    gresid, gup, gdown, gogate, gigate, gcin, gwout,
     rows, grads, hidden, d_gate, d_up, sel, send_rows, send_grads,
     part, sib, pairsum, plane, zsend, ret, dn, edge_out, edge_in, grx, mixed,
-    send_sem, recv_sem, in_sem, out_sem,
+    send_sem, recv_sem, in_sem,
 ):
     sp, tp, z, y, x, c = place()
     pairs = slices // 2
@@ -210,9 +209,9 @@
     ready = greet(sp_peers + [sibling, x_peer, diagonal])
 
     def pair_of(k):
-        pair, bit = 0, 1
+        code, pair, bit = k ^ (k >> 1), 0, 1
         while bit < pairs:
-            pair = pair + bit * lax.rem(lax.rem(lax.div(z, bit), 2) + (k // bit) % 2, 2)
+            pair = pair + bit * lax.rem(lax.rem(lax.div(z, bit), 2) + (code // bit) % 2, 2)
             bit *= 2
         return pair
 
@@ -240,7 +239,7 @@
             )
         )
     ]
-    stored, unit_cols = [], gate.shape[1]
+    unit_cols = gate.shape[1]
     slots_used, leaving = [0], [[]]
 
     def units_of(ref):
@@ -272,11 +271,6 @@
         ).start()
         return batch
 
-    def store(src, dst):
-        copy = pltpu.make_async_copy(src, dst, out_sem.at[len(stored)])
-        copy.start()
-        stored.append(copy)
-
     def block(pair, yy, xx, cc):
         return (rows_of(2 * pair + yy, cap), columns_of(2 * xx + cc, width))
 
@@ -305,30 +299,7 @@
         sel[rows_of(e, cap), :] = pick
         return pick, slot_weight
 
-    arriving = {}
-    home = block(z, y, x, c)
-    for k in range(1, pairs):
-        e = pair_of(k)
-        pick, slot_weight = choose(e)
-        here = rows_of(e, cap)
-        send_rows[here, :] = jnp.dot(pick, normed, preferred_element_type=F32).astype(BF16)
-        send_grads[here, :] = (
-            slot_weight * jnp.dot(pick, cot, preferred_element_type=F32)
-        ).astype(BF16)
-        if k == 1:
-            ready()
-        for a, (src, dst) in enumerate(((send_rows, rows), (send_grads, grads))):
-            arriving[k, a] = send(src.at[here, :], dst.at[home], (2 * e + y, tp))
-    pick, slot_weight = choose(z)
-    own_rows = rows_of(sp, cap)
-    rows[own_rows, :] = jnp.dot(
-        pick, (r32 * inv_rms).astype(BF16), preferred_element_type=F32
-    ).astype(BF16)
-    grads[own_rows, :] = (
-        slot_weight * jnp.dot(pick, og[...], preferred_element_type=F32)
-    ).astype(BF16)
-
-    both = (rows, grads)
+    both, arriving = (rows, grads), {}
     outs = [{} for _ in range(pairs)]
     near_rows = [Batch() for _ in range(pairs)]
 
@@ -340,6 +311,32 @@
         out["y", a] = send(ref.at[at], ref.at[at], y_peer)
         if k:
             send(ref.at[at], ref.at[at], sibling, near_rows[k])
+
+    def dispatch(k):
+        e = pair_of(k)
+        pick, slot_weight = choose(e)
+        here, home = rows_of(e, cap), block(z, y, x, c)
+        send_rows[here, :] = jnp.dot(pick, normed, preferred_element_type=F32).astype(BF16)
+        arriving[k, 0] = send(send_rows.at[here, :], rows.at[home], (2 * e + y, tp))
+        send_grads[here, :] = (
+            slot_weight * jnp.dot(pick, cot, preferred_element_type=F32)
+        ).astype(BF16)
+        arriving[k, 1] = send(send_grads.at[here, :], grads.at[home], (2 * e + y, tp))
+
+    pick, slot_weight = choose(z)
+    own_rows = rows_of(sp, cap)
+    rows[own_rows, :] = jnp.dot(
+        pick, (r32 * inv_rms).astype(BF16), preferred_element_type=F32
+    ).astype(BF16)
+    ready()
+    spread(0, 0)
+    dispatch(1)
+    grads[own_rows, :] = (
+        slot_weight * jnp.dot(pick, og[...], preferred_element_type=F32)
+    ).astype(BF16)
+    spread(0, 1)
+    for k in range(2, pairs):
+        dispatch(k)
 
     def got_x(k, a):
         out, ref, at = outs[k], both[a], block(pair_of(k), y, 1 - x, c)
@@ -383,36 +380,34 @@
             ).astype(BF16)
             d_up[at, :] = (d_hidden * activated).astype(BF16)
 
-    def partials(k, h):
-        at = rows_of(pair_of(k), 2 * cap)
-        cols = slice(2 * h * width, 2 * (h + 1) * width)
+    def partials(k, step):
+        at, h = rows_of(pair_of(k), 2 * cap), x if step else 1 - x
+        cols = columns_of(h, 2 * width)
         part[at, cols] = (
             lax.dot_general(
                 d_gate[at, :], gate[cols, :], across_units, preferred_element_type=F32
             )
             + lax.dot_general(d_up[at, :], up[cols, :], across_units, preferred_element_type=F32)
         ).astype(BF16)
-        halves[k, h] = send(
+        halves[k, step] = send(
             part.at[at, columns_of(2 * h + 1 - c, width)], sib.at[h, at, :], sibling
         )
 
-    def reduce_cores(k):
-        pair = pair_of(k)
+    def reduce_cores(k, step):
+        pair, h = pair_of(k), x if step else 1 - x
         at = rows_of(pair, 2 * cap)
-        for h in range(2):
-            halves[k, h].wait_recv()
-            pairsum[h, at, :] = (
-                part[at, columns_of(2 * h + c, width)].astype(F32) + sib[h, at, :].astype(F32)
-            ).astype(BF16)
+        halves[k, step].wait_recv()
+        pairsum[h, at, :] = (
+            part[at, columns_of(2 * h + c, width)].astype(F32) + sib[h, at, :].astype(F32)
+        ).astype(BF16)
         same, other = rows_of(2 * pair + y, cap), rows_of(2 * pair + 1 - y, cap)
         slots = rows_of(pair, cap)
-        moved[k] = Batch()
-        for n, src, peer in (
-            (2, pairsum.at[1 - x, other, :], diagonal),
-            (0, pairsum.at[1 - x, same, :], x_peer),
-            (1, pairsum.at[x, other, :], y_peer),
-        ):
-            send(src, plane.at[n, slots, :], peer, moved[k])
+        if step:
+            send(pairsum.at[h, other, :], plane.at[1, slots, :], y_peer, moved[k])
+        else:
+            moved[k] = Batch()
+            send(pairsum.at[h, other, :], plane.at[2, slots, :], diagonal, moved[k])
+            send(pairsum.at[h, same, :], plane.at[0, slots, :], x_peer, moved[k])
 
     def reduce_plane(k):
         pair = pair_of(k)
@@ -437,14 +432,12 @@
         gdown[at, :] = lax.dot_general(
             hidden[:, at], grads[...], over_rows, preferred_element_type=F32
         ).astype(BF16)
-        store(gdown.at[at, :], gdown_hbm.at[at, :])
 
     def up_chunk(n):
         at = slice(n * features // 4, (n + 1) * features // 4)
         gup[at, :] = lax.dot_general(
             rows[:, at], d_up[...], over_rows, preferred_element_type=F32
         ).astype(BF16)
-        store(gup.at[at, :], gup_hbm.at[at, :])
 
     own = rows_of(sp, tok)
 
@@ -464,8 +457,6 @@
             at = rows_of(2 * pair_of(k) + y, tok)
             send(mixed.at[at, :], mixed.at[at, :], y_peer, mixed_y)
 
-    for a in range(2):
-        spread(0, a)
     for a in range(2):
         got_y(0, a)
         spread(1, a)
@@ -493,27 +484,37 @@
         got_x(k, 1)
         if k + 2 == pairs:
             share_mixed()
+        if k + 1 == pairs:
+            for n in range(1, k - 1):
+                reduce_cores(n, 0)
+                reduce_cores(n, 1)
         experts(k - 1, 2)
         partials(k - 1, 0)
         got_d(k, 0)
         got_d(k, 1)
         partials(k - 1, 1)
-    for k in range(1, pairs - 1):
-        reduce_cores(k)
-    for step in range(3):
-        experts(pairs - 1, step)
-    for h in range(2):
-        partials(pairs - 1, h)
-    reduce_plane(1)
-    down_chunk(0)
-    reduce_cores(pairs - 1)
-    reduce_cores(0)
-    down_chunk(1)
-    for k in range(2, pairs - 1):
+    last = pairs - 1
+    experts(last, 0)
+    reduce_cores(last - 1, 0)
+    experts(last, 1)
+    reduce_cores(last - 1, 1)
+    experts(last, 2)
+    partials(last, 0)
+    partials(last, 1)
+    for k in range(1, last - 1):
         reduce_plane(k)
     up_chunk(0)
+    reduce_cores(last, 0)
+    reduce_cores(last, 1)
+    reduce_cores(0, 0)
+    reduce_cores(0, 1)
+    reduce_plane(last - 1)
     up_chunk(1)
-    reduce_plane(pairs - 1)
+    down_chunk(0)
+    down_chunk(1)
+    up_chunk(2)
+    up_chunk(3)
+    reduce_plane(last)
     reduce_plane(0)
     relay_mixed()
 
@@ -523,40 +524,42 @@
     ).astype(BF16)
     half, quarter = tok // 2, tok // 4
     far = columns_of(2 * (1 - x) + c, width)
-    tops = [slice(h * half, (h + 1) * half) for h in range(2)]
-    shares = [send(dn.at[at, mine], dn.at[at, mine], x_peer) for at in tops]
-    near = [send(dn.at[at, mine], dn.at[at, mine], sibling) for at in tops]
     share = features // slices
-    across = []
-
-    def share_rows(h):
-        shares[h].wait_recv()
-        send(dn.at[tops[h], far], dn.at[tops[h], far], sibling, near[h])
-        if h == 0:
-            up_chunk(2)
-        near[h].wait_recv()
-
-    def resid_rows(h):
-        at = tops[h]
-        unit = r32[at] * inv_rms[at]
+    shares, near, across, crossed = [], [], [], []
+    for h in (1 - x, x):
+        at = rows_of(h, half)
+        shares.append(send(dn.at[at, mine], dn.at[at, mine], x_peer))
+    for h in (x, 1 - x):
+        at = rows_of(h, half)
+        near.append(send(dn.at[at, mine], dn.at[at, mine], sibling))
+
+    def share_rows(step):
+        at = rows_of(1 - x if step else x, half)
+        shares[step].wait_recv()
+        send(dn.at[at, far], dn.at[at, far], sibling, near[step])
+        near[step].wait_recv()
+
+    def resid_rows(step):
+        at = rows_of(1 - x if step else x, half)
+        r_part = resid[at, :].astype(F32)
+        inv_part = lax.rsqrt(jnp.mean(r_part * r_part, axis=-1, keepdims=True) + epsilon)
+        unit = r_part * inv_part
         d_normed = dn[at, :].astype(F32)
         row_mean = jnp.mean(unit * d_normed, axis=-1, keepdims=True)
         gresid[at, :] = (
-            og[at, :].astype(F32) + inv_rms[at] * (d_normed - unit * row_mean)
+            og[at, :].astype(F32) + inv_part * (d_normed - unit * row_mean)
         ).astype(BF16)
-        for peer in sp_peers:
-            across.append(
-                send(
-                    gresid.at[rows_of(2 * h + c, quarter), columns_of(peer[0], share)],
-                    grx.at[rows_of(4 * sp + 2 * h + c, quarter), :], peer,
-                )
-            )
+
+    def piece(origin, xx):
+        return grx.at[rows_of(4 * origin + 2 * xx + c, quarter), :]
 
     share_rows(0)
     resid_rows(0)
+    for peer in sp_peers:
+        src = gresid.at[rows_of(2 * x + c, quarter), columns_of(peer[0], share)]
+        across.append(send(src, piece(sp, x), peer))
     share_rows(1)
     resid_rows(1)
-    store(gresid, gresid_hbm)
     d_mix = lax.dot_general(
         gresid[...], wout[...], (((1,), (1,)), ((), ())), preferred_element_type=F32
     )
@@ -567,15 +570,17 @@
     send(edge_out.at[0], edge_in.at[0], sp_peers[0], edges)
     send(edge_out.at[1], edge_in.at[1], sp_peers[-1], edges)
     gogate[...] = (d_mix * cout[...].astype(F32)).astype(BF16)
-    store(gogate, gogate_hbm)
     grx[own, :] = gresid[:, columns_of(sp, share)]
-    up_chunk(3)
-    for h in range(2):
-        for n in range(slices - 1):
-            across[h * (slices - 1) + n].wait_recv()
-            origin = lax.rem(sp + slices - 1 - n, slices)
-            got = grx.at[rows_of(4 * origin + 2 * h + c, quarter), :]
-            send(got, got, sibling, passed)
+    origins = [lax.rem(sp + slices - 1 - n, slices) for n in range(slices - 1)]
+    for n, origin in enumerate(origins):
+        across[n].wait_recv()
+        got = piece(origin, x)
+        crossed.append(send(got, got, x_peer))
+        send(got, got, sibling, passed)
+    for n, origin in enumerate(origins):
+        crossed[n].wait_recv()
+        got = piece(origin, 1 - x)
+        send(got, got, sibling, passed)
     edges.wait_recv()
     before = jnp.where(sp > 0, edge_in[0, 7:8, :], 0.0)
     after = jnp.where(sp < slices - 1, edge_in[1, 0:1, :], 0.0)
@@ -584,17 +589,12 @@
     former = jnp.where(at == 0, before, pltpu.roll(d_conv, 1, 0))
     d_inner = taps[0:1, :] * later + taps[1:2, :] * d_conv + taps[2:3, :] * former
     gigate[...] = (d_inner * cin[...].astype(F32)).astype(BF16)
-    store(gigate, gigate_hbm)
     gcin[...] = (d_inner * igate[...].astype(F32)).astype(BF16)
-    store(gcin, gcin_hbm)
     passed.wait_recv()
     mixed_y.wait_recv()
     gwout[...] = lax.dot_general(grx[...], mixed[...], over_rows, preferred_element_type=F32)
-    store(gwout, gwout_hbm)
     for n, units in enumerate(leaving):
         await_units(send_sem.at[n], sum(units))
-    for copy in stored:
-        copy.wait()
     assert slots_used[0] == recv_sem.shape[0] and len(leaving) <= send_sem.shape[0]
 
 
@@ -603,7 +603,7 @@
     tok, features = resid.shape
     units, channels = gate.shape[1], ogate.shape[1]
     pairs, width = slices // 2, features // 4
-    anywhere = pl.BlockSpec(memory_space=pl.ANY)
+    anywhere = pl.BlockSpec(memory_space=pltpu.HBM)
     share = features // slices
     outs = (
         (resid.shape, BF16), (gate.shape, BF16), (down.shape, BF16),
@@ -613,11 +613,10 @@
     sems = 12 * pairs + 2 * slices + 3
     return pl.pallas_call(
         functools.partial(layer_kernel, slices, cap),
-        out_shape=tuple(jax.ShapeDtypeStruct(*out) for out in outs),
+        out_shape=tuple(pltpu.VMEM(*out) for out in outs),
         in_specs=[anywhere] * len(args),
-        out_specs=[anywhere] * len(outs),
+        out_specs=[pl.BlockSpec(memory_space=pltpu.VMEM)] * len(outs),
         scratch_shapes=[pltpu.VMEM(arg.shape, arg.dtype) for arg in args]
-        + [pltpu.VMEM(*out) for out in outs]
         + [
             pltpu.VMEM((rows, features), BF16),
             pltpu.VMEM((rows, features), BF16),
@@ -641,50 +640,33 @@
             pltpu.SemaphoreType.DMA((5,)),
             pltpu.SemaphoreType.DMA((sems,)),
             pltpu.SemaphoreType.DMA((len(args),)),
-            pltpu.SemaphoreType.DMA((len(outs) + 4,)),
         ],
         compiler_params=pltpu.CompilerParams(
-            collective_id=0, has_side_effects=True, vmem_limit_bytes=VMEM_LIMIT
+            collective_id=0, has_side_effects=True, vmem_limit_bytes=VMEM_LIMIT // 2
         ),
         name="layer",
-    )(*args)
-
-
-def publish_kernel(count, chunks, *refs):
-    srcs, dsts, held = refs[:count], refs[count : 2 * count], refs[2 * count : 3 * count]
-    in_sem, out_sem = refs[3 * count :]
-    pieces = []
-    for src, dst, buf, cut in zip(srcs, dsts, held, chunks):
-        height = src.shape[0] // cut
-        for n in range(cut):
-            at = pl.ds(n * height, height)
-            i = len(pieces)
-            pieces.append(
-                (
-                    pltpu.make_async_copy(src.at[at, :], buf.at[at, :], in_sem.at[i]),
-                    pltpu.make_async_copy(buf.at[at, :], dst.at[at, :], out_sem.at[i]),
-                )
-            )
-    for take, _ in pieces:
-        take.start()
-    for take, give in pieces:
-        take.wait()
-        give.start()
-    for _, give in pieces:
-        give.wait()
+    )(*(pltpu.with_memory_space_constraint(arg, pltpu.HBM) for arg in args))
+
+
+def publish_kernel(count, *refs):
+    copies = [
+        pltpu.make_async_copy(src, dst, refs[-1].at[n])
+        for n, (src, dst) in enumerate(zip(refs[:count], refs[count : 2 * count]))
+    ]
+    for copy in copies:
+        copy.start()
+    for copy in copies:
+        copy.wait()
 
 
 def publish(arrays):
-    chunks = [max(1, a.size * a.dtype.itemsize // (512 * 1024)) for a in arrays]
-    anywhere = pl.BlockSpec(memory_space=pl.ANY)
     return pl.pallas_call(
-        functools.partial(publish_kernel, len(arrays), chunks),
+        functools.partial(publish_kernel, len(arrays)),
         out_shape=tuple(jax.ShapeDtypeStruct(a.shape, a.dtype) for a in arrays),
-        in_specs=[anywhere] * len(arrays),
-        out_specs=[anywhere] * len(arrays),
-        scratch_shapes=[pltpu.VMEM(a.shape, a.dtype) for a in arrays]
-        + [pltpu.SemaphoreType.DMA((sum(chunks),))] * 2,
-        compiler_params=pltpu.CompilerParams(vmem_limit_bytes=VMEM_LIMIT),
+        in_specs=[pl.BlockSpec(memory_space=pltpu.VMEM)] * len(arrays),
+        out_specs=[pl.BlockSpec(memory_space=pl.ANY)] * len(arrays),
+        scratch_shapes=[pltpu.SemaphoreType.DMA((len(arrays),))],
+        compiler_params=pltpu.CompilerParams(vmem_limit_bytes=VMEM_LIMIT // 4),
         name="publish",
     )(*arrays)
 

time: 73.9 us -> 68.9 us (0.932)
  Pallas kernels: 73.1 us -> 68.1 us
    pallas_call x1, Pallas kernels: 68.5 us -> 65.7 us  [layer(): pl.pallas_call(functools.partial(layer_kernel, slices, cap), out_shape=tu...]
    pallas_call x1, Pallas kernels: 4.59 us -> 2.38 us  [publish(): pl.pallas_call(functools.partial(publish_kernel, len(arrays)), out_shape=...]
where the time goes in v3:
time: 68.9 us; the launch traced here: 68.8 us
  Pallas kernels  68.1 us (99%)
    pallas_call x1, Pallas kernels, layer(): pl.pallas_call(functools.partial(layer_kernel, slices, cap), out_shape=tu...  65.7 us
    pallas_call x1, Pallas kernels, publish(): pl.pallas_call(functools.partial(publish_kernel, len(arrays)), out_shape=...  2.38 us

profile of v3, /device:TPU:0, one launch (start us, length us, event | category | flops | bytes accessed | tf_op | source)
XLA Modules:
  0.0 68.8 jit_solution(10756100920392486763)
XLA Ops:
  0.6 65.7 %layer.1 = (bf16[128,2048]{1,0:T(8,128)(2,1)S(1)}, bf16[2048,512]{1,0:T(8,128)(2,1)S(1)}, bf16[512,2048]{1,0:T(8,128)(2,1)S(1)}, bf16[128,256]{1,0:T(8,128)(2,1)...) custom-call(s32[2,128]{1,0:T(2,128)} %bitcast.10, f32[2,128]{1,0:T(2,128)} %bitcast.11, ...), custom_call_target="tpu_custom_call" | custom-call | tf_op jit(solution)/shard_map/layer/pallas_call | solution.py:614
  66.4 2.4 %publish.1 = (bf16[128,2048]{1,0:T(8,128)(2,1)}, bf16[2048,512]{1,0:T(8,128)(2,1)}, bf16[512,2048]{1,0:T(8,128)(2,1)}, bf16[128,256]{1,0:T(8,128)(2,1)}, bf16[12...) custom-call(bf16[128,2048]{1,0:T(8,128)(2,1)S(1)} %get-tuple-element.21.refs_0_, ...), custom_call_target="tpu_custom_call" | custom-call | tf_op jit(solution)/shard_map/publish/pallas_call | solution.py:663

commit v4 on v3

--- a/solution.py
+++ b/solution.py
@@ -193,7 +193,7 @@
     gresid, gup, gdown, gogate, gigate, gcin, gwout,
     rt, rw, resid, og, gate, up, down, ogate, igate, cin, cout, taps, wout,
     rows, grads, hidden, d_gate, d_up, sel, send_rows, send_grads,
-    part, sib, pairsum, plane, zsend, ret, dn, edge_out, edge_in, grx, mixed,
+    gate_t, up_t, down_t, part, sib, pairsum, plane, zsend, ret, dn, edge_out, edge_in, grx, mixed,
     send_sem, recv_sem, in_sem,
 ):
     sp, tp, z, y, x, c = place()
@@ -204,9 +204,10 @@
     sibling = (sp, 2 * x + 1 - c)
     x_peer = (sp, 2 * (1 - x) + c)
     y_peer = (2 * z + 1 - y, tp)
+    x_other = (sp, 2 * (1 - x) + 1 - c)
     diagonal = (2 * z + 1 - y, 2 * (1 - x) + c)
     sp_peers = [(lax.rem(sp + k, slices), tp) for k in range(1, slices)]
-    ready = greet(sp_peers + [sibling, x_peer, diagonal])
+    ready = greet(sp_peers + [sibling, x_peer, x_other, diagonal])
 
     def pair_of(k):
         code, pair, bit = k ^ (k >> 1), 0, 1
@@ -228,7 +229,7 @@
     ]
     weights = [
         fetch(4 + n, src, dst)
-        for n, (src, dst) in enumerate(((gate_hbm, gate), (up_hbm, up), (down_hbm, down)))
+        for n, (src, dst) in enumerate(((down_hbm, down), (gate_hbm, gate), (up_hbm, up)))
     ]
     gates = [
         fetch(7 + n, src, dst)
@@ -311,6 +312,9 @@
         out["y", a] = send(ref.at[at], ref.at[at], y_peer)
         if k:
             send(ref.at[at], ref.at[at], sibling, near_rows[k])
+        elif a == 0:
+            at = block(z, y, 1 - x, c)
+            out["d", a] = send(ref.at[at], ref.at[at], y_peer)
 
     def dispatch(k):
         e = pair_of(k)
@@ -325,16 +329,16 @@
 
     pick, slot_weight = choose(z)
     own_rows = rows_of(sp, cap)
+    grads[own_rows, :] = (
+        slot_weight * jnp.dot(pick, og[...], preferred_element_type=F32)
+    ).astype(BF16)
+    ready()
+    spread(0, 1)
+    dispatch(1)
     rows[own_rows, :] = jnp.dot(
         pick, (r32 * inv_rms).astype(BF16), preferred_element_type=F32
     ).astype(BF16)
-    ready()
     spread(0, 0)
-    dispatch(1)
-    grads[own_rows, :] = (
-        slot_weight * jnp.dot(pick, og[...], preferred_element_type=F32)
-    ).astype(BF16)
-    spread(0, 1)
     for k in range(2, pairs):
         dispatch(k)
 
@@ -348,7 +352,7 @@
     def got_y(k, a):
         out, ref, at = outs[k], both[a], block(pair_of(k), 1 - y, x, c)
         out["y", a].wait_recv()
-        if k == 0 or a == 1:
+        if a == 1:
             out["d", a] = send(ref.at[at], ref.at[at], x_peer)
         send(ref.at[at], ref.at[at], sibling, near_rows[k])
 
@@ -357,7 +361,6 @@
         out["d", a].wait_recv()
         send(ref.at[at], ref.at[at], sibling, near_rows[k])
 
-    across_units = (((1,), (1,)), ((), ()))
     held, halves, moved, back = {}, {}, {}, Batch()
 
     def experts(k, step):
@@ -369,9 +372,7 @@
             held["up"] = jnp.dot(rows[at, :], up[...], preferred_element_type=F32)
         else:
             pre_gate, pre_up = held["gate"], held["up"]
-            d_hidden = lax.dot_general(
-                grads[at, :], down[...], across_units, preferred_element_type=F32
-            )
+            d_hidden = jnp.dot(grads[at, :], down_t[...], preferred_element_type=F32)
             sigmoid_gate = jax.nn.sigmoid(pre_gate)
             activated = pre_gate * sigmoid_gate
             hidden[at, :] = (activated * pre_up).astype(BF16)
@@ -384,10 +385,8 @@
         at, h = rows_of(pair_of(k), 2 * cap), x if step else 1 - x
         cols = columns_of(h, 2 * width)
         part[at, cols] = (
-            lax.dot_general(
-                d_gate[at, :], gate[cols, :], across_units, preferred_element_type=F32
-            )
-            + lax.dot_general(d_up[at, :], up[cols, :], across_units, preferred_element_type=F32)
+            jnp.dot(d_gate[at, :], gate_t[:, cols], preferred_element_type=F32)
+            + jnp.dot(d_up[at, :], up_t[:, cols], preferred_element_type=F32)
         ).astype(BF16)
         halves[k, step] = send(
             part.at[at, columns_of(2 * h + 1 - c, width)], sib.at[h, at, :], sibling
@@ -457,46 +456,67 @@
             at = rows_of(2 * pair_of(k) + y, tok)
             send(mixed.at[at, :], mixed.at[at, :], y_peer, mixed_y)
 
-    for a in range(2):
-        got_y(0, a)
-        spread(1, a)
-    for copy in weights:
-        copy.wait()
+    def turn(n):
+        weights[n].wait()
+        src, dst = ((down, down_t), (gate, gate_t), (up, up_t))[n]
+        dst[...] = src[...].T
+
+    turn(0)
+    got_y(0, 1)
+    spread(1, 0)
+    spread(1, 1)
+    got_y(0, 0)
+    turn(1)
+    last = pairs - 1
     for k in range(1, pairs):
         if k == 1:
             got_d(0, 0)
-        got_y(k, 0)
-        if k == 1:
+            got_y(k, 0)
             got_x(k, 0)
             got_y(k, 1)
             got_d(0, 1)
-        if k + 1 < pairs:
-            spread(k + 1, 0)
-        experts(k - 1, 0)
-        if k > 1:
+            turn(2)
+            spread(2, 0)
+            spread(2, 1)
+            got_x(k, 1)
+            experts(k - 1, 0)
+            experts(k - 1, 1)
+        elif k == 2:
+            got_y(k, 0)
+            experts(k - 1, 0)
+            got_x(k, 0)
             got_y(k, 1)
+            experts(k - 1, 1)
+            got_x(k, 1)
+        else:
+            got_y(k, 0)
             got_x(k, 0)
-        elif k + 1 < pairs:
-            spread(k + 1, 1)
-        experts(k - 1, 1)
-        if 1 < k < pairs - 1:
-            spread(k + 1, 1)
-        got_x(k, 1)
+            got_y(k, 1)
+            got_x(k, 1)
+            got_d(k - 1, 0)
+            got_d(k - 1, 1)
+            reduce_cores(k - 2, 0)
+            reduce_cores(k - 2, 1)
+            experts(k - 1, 0)
+            experts(k - 1, 1)
+        if k == last:
+            got_d(k, 0)
+            got_d(k, 1)
+        if k + 2 < pairs:
+            spread(k + 2, 0)
         if k + 2 == pairs:
             share_mixed()
-        if k + 1 == pairs:
-            for n in range(1, k - 1):
-                reduce_cores(n, 0)
-                reduce_cores(n, 1)
         experts(k - 1, 2)
         partials(k - 1, 0)
-        got_d(k, 0)
-        got_d(k, 1)
+        if k + 2 < pairs:
+            spread(k + 2, 1)
+        if k == 1:
+            got_d(k, 0)
+            got_d(k, 1)
         partials(k - 1, 1)
-    last = pairs - 1
     experts(last, 0)
+    experts(last, 1)
     reduce_cores(last - 1, 0)
-    experts(last, 1)
     reduce_cores(last - 1, 1)
     experts(last, 2)
     partials(last, 0)
@@ -508,13 +528,13 @@
     reduce_cores(last, 1)
     reduce_cores(0, 0)
     reduce_cores(0, 1)
-    reduce_plane(last - 1)
     up_chunk(1)
     down_chunk(0)
+    reduce_plane(last - 1)
     down_chunk(1)
+    reduce_plane(last)
     up_chunk(2)
     up_chunk(3)
-    reduce_plane(last)
     reduce_plane(0)
     relay_mixed()
 
@@ -523,24 +543,16 @@
         sel[...], ret[...], over_rows, preferred_element_type=F32
     ).astype(BF16)
     half, quarter = tok // 2, tok // 4
-    far = columns_of(2 * (1 - x) + c, width)
+    far, beyond = columns_of(2 * (1 - x) + c, width), columns_of(1 - x, 2 * width)
     share = features // slices
-    shares, near, across, crossed = [], [], [], []
-    for h in (1 - x, x):
-        at = rows_of(h, half)
-        shares.append(send(dn.at[at, mine], dn.at[at, mine], x_peer))
-    for h in (x, 1 - x):
-        at = rows_of(h, half)
-        near.append(send(dn.at[at, mine], dn.at[at, mine], sibling))
-
-    def share_rows(step):
-        at = rows_of(1 - x if step else x, half)
-        shares[step].wait_recv()
-        send(dn.at[at, far], dn.at[at, far], sibling, near[step])
-        near[step].wait_recv()
-
-    def resid_rows(step):
-        at = rows_of(1 - x if step else x, half)
+    leading, trailing = Batch(), Batch()
+    here, there = rows_of(2 * x + c, quarter), rows_of(2 * x + 1 - c, quarter)
+    away = rows_of(1 - x, half)
+
+    def share_rows(at, cols, peer, batch=None):
+        return send(dn.at[at, cols], dn.at[at, cols], peer, batch)
+
+    def resid_rows(at):
         r_part = resid[at, :].astype(F32)
         inv_part = lax.rsqrt(jnp.mean(r_part * r_part, axis=-1, keepdims=True) + epsilon)
         unit = r_part * inv_part
@@ -550,36 +562,53 @@
             og[at, :].astype(F32) + inv_part * (d_normed - unit * row_mean)
         ).astype(BF16)
 
+    share_rows(rows_of(2 * (1 - x) + 1 - c, quarter), mine, x_other, leading)
+    share_rows(rows_of(2 * (1 - x) + c, quarter), mine, x_peer, leading)
+    share_rows(there, mine, sibling, leading)
+    rest = share_rows(rows_of(x, half), mine, x_peer)
+    share_rows(here, mine, sibling, trailing)
+    share_rows(away, mine, sibling, trailing)
+
     def piece(origin, xx):
         return grx.at[rows_of(4 * origin + 2 * xx + c, quarter), :]
 
-    share_rows(0)
-    resid_rows(0)
-    for peer in sp_peers:
-        src = gresid.at[rows_of(2 * x + c, quarter), columns_of(peer[0], share)]
-        across.append(send(src, piece(sp, x), peer))
-    share_rows(1)
-    resid_rows(1)
+    def peer_of(j, flip):
+        return 2 * pair_of(j) + (1 - y if flip else y)
+
+    leading.wait_recv()
+    resid_rows(here)
+    across, crossed, passed = {}, {}, Batch()
+    for j, flip in [(j, f) for j in range(pairs - 1, 0, -1) for f in range(2)] + [(0, 1)]:
+        peer = peer_of(j, flip)
+        src = gresid.at[here, columns_of(peer, share)]
+        across[j, flip] = send(src, piece(sp, x), (peer, tp))
+    share_rows(here, beyond, sibling, trailing)
+    rest.wait_recv()
+    share_rows(away, far, sibling, trailing)
+    trailing.wait_recv()
+    resid_rows(there)
+    resid_rows(away)
     d_mix = lax.dot_general(
         gresid[...], wout[...], (((1,), (1,)), ((), ())), preferred_element_type=F32
     )
     d_conv = d_mix * ogate[...].astype(F32)
     edge_out[0] = d_conv[tok - 8 :]
     edge_out[1] = d_conv[:8]
-    edges, passed = Batch(), Batch()
+    edges = Batch()
     send(edge_out.at[0], edge_in.at[0], sp_peers[0], edges)
     send(edge_out.at[1], edge_in.at[1], sp_peers[-1], edges)
     gogate[...] = (d_mix * cout[...].astype(F32)).astype(BF16)
     grx[own, :] = gresid[:, columns_of(sp, share)]
-    origins = [lax.rem(sp + slices - 1 - n, slices) for n in range(slices - 1)]
-    for n, origin in enumerate(origins):
-        across[n].wait_recv()
-        got = piece(origin, x)
-        crossed.append(send(got, got, x_peer))
+    arrivals = [(0, 1), (1, 0), (1, 1)]
+    arrivals += [(j, f) for j in range(pairs - 1, 1, -1) for f in range(2)]
+    for j, flip in arrivals:
+        across[j, flip].wait_recv()
+        got = piece(peer_of(j, flip), x)
+        crossed[j, flip] = send(got, got, x_peer)
         send(got, got, sibling, passed)
-    for n, origin in enumerate(origins):
-        crossed[n].wait_recv()
-        got = piece(origin, 1 - x)
+    for j, flip in arrivals:
+        crossed[j, flip].wait_recv()
+        got = piece(peer_of(j, flip), 1 - x)
         send(got, got, sibling, passed)
     edges.wait_recv()
     before = jnp.where(sp > 0, edge_in[0, 7:8, :], 0.0)
@@ -610,7 +639,7 @@
         (ogate.shape, BF16), (ogate.shape, BF16), (ogate.shape, BF16), ((share, channels), F32),
     )
     rows = slices * cap
-    sems = 12 * pairs + 2 * slices + 3
+    sems = 12 * pairs + 2 * slices + 2
     return pl.pallas_call(
         functools.partial(layer_kernel, slices, cap),
         out_shape=tuple(pltpu.VMEM(*out) for out in outs),
@@ -626,6 +655,9 @@
             pltpu.VMEM((pairs * cap, tok), BF16),
             pltpu.VMEM((pairs * cap, width), BF16),
             pltpu.VMEM((pairs * cap, width), BF16),
+            pltpu.VMEM((units, features), BF16),
+            pltpu.VMEM((units, features), BF16),
+            pltpu.VMEM((features, units), BF16),
             pltpu.VMEM((rows, features), BF16),
             pltpu.VMEM((2, rows, width), BF16),
             pltpu.VMEM((2, rows, width), BF16),
@@ -642,7 +674,7 @@
             pltpu.SemaphoreType.DMA((len(args),)),
         ],
         compiler_params=pltpu.CompilerParams(
-            collective_id=0, has_side_effects=True, vmem_limit_bytes=VMEM_LIMIT // 2
+            collective_id=0, has_side_effects=True, vmem_limit_bytes=2 * VMEM_LIMIT // 3
         ),
         name="layer",
     )(*(pltpu.with_memory_space_constraint(arg, pltpu.HBM) for arg in args))

time: 68.9 us -> 64.9 us (0.942)
  Pallas kernels: 68.1 us -> 63.6 us
    pallas_call x1, Pallas kernels: 65.7 us -> 61.2 us  [layer(): pl.pallas_call(functools.partial(layer_kernel, slices, cap), out_shape=tu...]
where the time goes in v4:
time: 64.9 us; the launch traced here: 64.4 us
  Pallas kernels  63.6 us (98%)
  between operations  0.81 us (1%)
    pallas_call x1, Pallas kernels, layer(): pl.pallas_call(functools.partial(layer_kernel, slices, cap), out_shape=tu...  61.2 us
    pallas_call x1, Pallas kernels, publish(): pl.pallas_call(functools.partial(publish_kernel, len(arrays)), out_shape=...  2.38 us

profile of v4, /device:TPU:0, one launch (start us, length us, event | category | flops | bytes accessed | tf_op | source)
XLA Modules:
  0.0 64.4 jit_solution(212357200514832248)
XLA Ops:
  0.6 61.2 %layer.1 = (bf16[128,2048]{1,0:T(8,128)(2,1)S(1)}, bf16[2048,512]{1,0:T(8,128)(2,1)S(1)}, bf16[512,2048]{1,0:T(8,128)(2,1)S(1)}, bf16[128,256]{1,0:T(8,128)(2,1)...) custom-call(s32[2,128]{1,0:T(2,128)} %bitcast.10, f32[2,128]{1,0:T(2,128)} %bitcast.11, ...), custom_call_target="tpu_custom_call" | custom-call | tf_op jit(solution)/shard_map/layer/pallas_call | solution.py:643
  61.9 2.4 %publish.1 = (bf16[128,2048]{1,0:T(8,128)(2,1)}, bf16[2048,512]{1,0:T(8,128)(2,1)}, bf16[512,2048]{1,0:T(8,128)(2,1)}, bf16[128,256]{1,0:T(8,128)(2,1)}, bf16[12...) custom-call(bf16[128,2048]{1,0:T(8,128)(2,1)S(1)} %get-tuple-element.21.refs_0_, ...), custom_call_target="tpu_custom_call" | custom-call | tf_op jit(solution)/shard_map/publish/pallas_call | solution.py:695
